TPU v7x, 32 devices: a whole 2x2x4 slice. The times are simulated.
32 devices in a mesh: grp: 2 (over y), sp: 4 (over z), tp: 4 (over x, core).
Axes of the slice: x: 2, y: 2, z: 4, core: 2. Of those that a mesh axis runs over, the one named last changes fastest.
Arguments:
- queries: bfloat16 [4096, 1024], P(('grp', 'sp'), 'tp'), parts along dimension 0, may hold values from -120 to 120
- keys: bfloat16 [4096, 256], P(('grp', 'sp')), parts along dimension 0, may hold values from -6 to 6
- values: bfloat16 [4096, 256], P(('grp', 'sp')), parts along dimension 0, may hold values from -6 to 6
- sink: float32 [8], P('tp'), may hold values from 1 to 5
- resid: bfloat16 [4096, 2048], P(('grp', 'sp')), parts along dimension 0, may hold values from -100 to 100
- out_proj: bfloat16 [1024, 2048], P(None, 'tp'), may hold values from -1.5 to 1.5
- norm_gain: float32 [2048], replicated, may hold values from 0.1 to 1.9
- w_gate: bfloat16 [2048, 6144], P('sp', 'tp'), may hold values from -0.125 to 0.125
- w_up: bfloat16 [2048, 6144], P('sp', 'tp'), may hold values from -0.125 to 0.125
- conv_w: float32 [3, 6144], P(None, 'tp'), may hold values from -3 to 3
- conv_b: float32 [6144], P('tp'), may hold values from -3 to 3
- w_down: bfloat16 [6144, 2048], P('tp', 'sp'), may hold values from -0.21875 to 0.21875
Outputs:
- layer_out: bfloat16 [4096, 2048], P(('grp', 'sp'), 'tp'), parts along dimension 0
There are 2 independent parts, one for each index of `grp`. A program takes and returns all parts, laid end to end along the dimension named above; an argument that names none is the same for every part. Nothing has to cross between parts.
All inputs are finite; a program needn't handle non-finite values.
Results may differ from a plain program's by a relative error of at most 0.015.
Values may be sent and summed in bfloat16 or wider, within the bound.
No kernel may reach another device: no remote copies, remote signals or barrier semaphores. Data moves between devices by JAX's collectives and lax.ppermute only.
A program may use at most 64 MiB of HBM per device.

v0:
```python
import jax
import jax.numpy as jnp
from jax import lax
from jax.sharding import PartitionSpec as P

H = 8
KVH = 2
HD = 128
WINDOW = 128
CONV = 3


def with_halo(cells, sides, width):
    for axis, dim in sides:
        count = lax.axis_size(axis)
        ends = count - 1
        head = lax.slice_in_dim(cells, 0, width, axis=dim)
        tail = lax.slice_in_dim(cells, cells.shape[dim] - width, cells.shape[dim], axis=dim)
        cells = jnp.concatenate(
            [
                lax.ppermute(tail, axis, [(i, (i + 1) % count) for i in range(ends)]),
                cells,
                lax.ppermute(head, axis, [((i + 1) % count, i) for i in range(ends)]),
            ],
            axis=dim,
        )
    return cells


def shards(
    queries, keys, values, sink, resid, out_proj, norm_gain, w_gate, w_up, conv_w, conv_b, w_down
):
    tokens = queries.shape[0]
    width = resid.shape[1]
    heads_here = sink.shape[0]
    group = H // KVH
    scale = HD ** (-0.5)
    first_head = lax.axis_index("tp") * heads_here
    kv_head = first_head // group
    own_keys = lax.dynamic_slice_in_dim(keys, kv_head * HD, HD, 1)
    own_values = lax.dynamic_slice_in_dim(values, kv_head * HD, HD, 1)
    extended = with_halo(jnp.stack([own_keys, own_values]), (("sp", 1),), WINDOW)
    ext_keys = extended[0]
    ext_values = extended[1]
    span = tokens + 2 * WINDOW
    q_heads = queries.reshape(tokens, heads_here, HD)
    scores = (
        jnp.einsum("qhd,kd->hqk", q_heads, ext_keys, preferred_element_type=jnp.float32) * scale
    )
    offset = lax.axis_index("sp") * tokens
    q_pos = offset + jnp.arange(tokens, dtype=jnp.int32)[:, None]
    k_pos = offset - WINDOW + jnp.arange(span, dtype=jnp.int32)[None, :]
    seq_total = tokens * lax.axis_size("sp")
    valid = (jnp.abs(q_pos - k_pos) <= WINDOW) & (k_pos >= 0) & (k_pos < seq_total)
    scores = jnp.where(valid[None], scores, jnp.float32(-1e30))
    sink_col = sink[:, None]
    top = jnp.maximum(jnp.max(scores, axis=-1), sink_col)
    expo = jnp.exp(scores - top[..., None])
    total = jnp.sum(expo, axis=-1) + jnp.exp(sink_col - top)
    weights = (expo / total[..., None]).astype(jnp.bfloat16)
    heads_out = jnp.einsum("hqk,kd->qhd", weights, ext_values, preferred_element_type=jnp.float32)
    heads_out = heads_out.astype(jnp.bfloat16).reshape(tokens, heads_here * HD)
    all_heads = lax.all_gather(heads_out, "tp", axis=1, tiled=True)
    cols = width // lax.axis_size("tp")
    col_start = lax.axis_index("tp") * cols
    full_proj = lax.all_gather(out_proj, "tp", axis=1, tiled=True)
    summed = resid.astype(jnp.float32) + jnp.dot(
        all_heads, full_proj, preferred_element_type=jnp.float32
    )
    mean = jnp.mean(summed, axis=-1, keepdims=True)
    msq = jnp.mean(summed * summed, axis=-1, keepdims=True)
    normed_full = ((summed - mean) * lax.rsqrt(msq - mean * mean + 1e-05) * norm_gain).astype(
        jnp.bfloat16
    )
    normed_own = lax.dynamic_slice_in_dim(normed_full, col_start, cols, 1)
    gate_acc = jnp.dot(
        normed_full,
        lax.all_gather(w_gate, "sp", axis=0, tiled=True),
        preferred_element_type=jnp.float32,
    )
    up_acc = jnp.dot(
        normed_full,
        lax.all_gather(w_up, "sp", axis=0, tiled=True),
        preferred_element_type=jnp.float32,
    )
    gate_pre = gate_acc.astype(jnp.bfloat16)
    up_part = up_acc.astype(jnp.bfloat16)
    padded = with_halo(gate_pre, (("sp", 0),), CONV // 2)
    conv = conv_b
    for tap in range(CONV):
        conv = conv + padded[tap : tap + tokens].astype(jnp.float32) * conv_w[tap]
    act = (jax.nn.silu(conv) * up_part.astype(jnp.float32)).astype(jnp.bfloat16)
    terms = jnp.dot(
        act, lax.all_gather(w_down, "sp", axis=1, tiled=True), preferred_element_type=jnp.float32
    )
    ffn_own = lax.psum_scatter(
        terms.astype(jnp.bfloat16), "tp", scatter_dimension=1, tiled=True
    ).astype(jnp.float32)
    return (normed_own.astype(jnp.float32) + ffn_own).astype(jnp.bfloat16)


def solution(mesh):
    return jax.shard_map(
        shards,
        mesh=mesh,
        in_specs=(
            P(("grp", "sp"), "tp"),
            P(("grp", "sp"), None),
            P(("grp", "sp"), None),
            P("tp"),
            P(("grp", "sp"), None),
            P(None, "tp"),
            P(),
            P("sp", "tp"),
            P("sp", "tp"),
            P(None, "tp"),
            P("tp"),
            P("tp", "sp"),
        ),
        out_specs=P(("grp", "sp"), "tp"),
        check_vma=False,
    )
```

profile of v0, /device:TPU:0, one launch (start us, length us, event | category | flops | bytes accessed | tf_op | source)
XLA Modules:
  0.0 476.0 jit_solution(9016852230966235995)
XLA Ops:
  6.5 1.0 dynamic-slice_bitcast_fusion
  7.6 5.0 %collective-permute-start = (bf16[2,128,128]{2,1,0:T(8,128)(2,1)S(1)}, bf16[2,128,128]{2,1,0:T(8,128)(2,1)S(1)}, u32[]{:S(2)}, u32[]{:S(2)}) collective-permute-start(bf16[2,128,128]{2,1,0:T(8,128)(2,1)S(1)} %get-tuple-element.12), channel_id=1, source_target_pairs={{0,4},{4,8},{8,12},{1,5},{5,9},{9,13},{2,6},{6,10},{10,14},{3,7},{... | collective-permute-start | bytes 196616 | tf_op jit(solution)/shard_map/ppermute | solution.py:21
  12.6 1.3 collective-permute-start.1
  13.9 0.8 fusion.10
  14.7 4.0 collective-permute-done.1
  18.8 0.8 fusion.1
  19.6 0.7 fusion
  20.4 1.9 fusion.12
  22.3 0.7 all-gather.8.cloned.1.call-update
  23.1 0.7 all-gather.10.cloned.1.call-update
  24.4 0.5 all-gather.14.cloned.1.call-update
  25.0 14.4 %all-gather.6.cloned.1.call-done = bf16[512,1024]{0,1:T(8,128)(2,1)} async-done(((bf16[512,256]{0,1:T(8,128)(2,1)}), bf16[512,1024]{0,1:T(8,128)(2,1)}) %all-gather.6.cloned.1.call-update) | async-done | bytes 1048592 | tf_op jit(solution)/shard_map/all_gather | solution.py:63
  39.4 36.0 %all-gather.8.cloned.1.call-done = bf16[1024,2048]{1,0:T(8,128)(2,1)} async-done(((bf16[1024,512]{1,0:T(8,128)(2,1)}), bf16[1024,2048]{1,0:T(8,128)(2,1)}) %all-gather.8.cloned.1.call-update) | async-done | bytes 4194320 | tf_op jit(solution)/shard_map/all_gather | solution.py:66
  75.4 5.4 %fusion.22 = (f32[512]{0:T(512)S(1)}, f32[512]{0:T(512)S(1)}, f32[512,2048]{1,0:T(8,128)S(1)}) fusion(bf16[512,1024]{0,1:T(8,128)(2,1)} %all-gather.6.cloned.1.call-done, bf16[1024,2048]{1,0:T(8,128)(2,1)} %all-gather.8.cloned.1.call-done, bf16[512,2048]{1,0:T(8,128)(2,1)S(1)} %copy-done.5), kind=kOutput, calls=%fused_computation.52 | convolution fusion | flops 2152725504 | bytes 11538432 | tf_op jit(solution)/shard_map/dot_general | solution.py:67
  80.8 0.6 multiply_convert_fusion
  81.5 110.9 %all-gather.10.cloned.1.call-done = bf16[2048,1536]{1,0:T(8,128)(2,1)} async-done(((bf16[512,1536]{1,0:T(8,128)(2,1)}), bf16[2048,1536]{1,0:T(8,128)(2,1)}) %all-gather.10.cloned.1.call-update) | async-done | bytes 6291472 | tf_op jit(solution)/shard_map/all_gather | solution.py:78
  192.4 6.2 %convolution_convert_fusion.2 = bf16[512,1536]{1,0:T(8,128)(2,1)S(1)} fusion(bf16[512,2048]{1,0:T(8,128)(2,1)S(1)} %multiply_convert_fusion, bf16[2048,1536]{1,0:T(8,128)(2,1)} %all-gather.10.cloned.1.call-done), kind=kOutput, calls=%fused_computation.9 | convolution fusion | flops 3222011904 | bytes 9961472 | tf_op jit(solution)/shard_map/dot_general | solution.py:76
  198.6 1.3 collective-permute-start.2
  199.9 1.5 collective-permute-start.3
  201.5 105.9 %all-gather.12.cloned.1.call-done = bf16[2048,1536]{1,0:T(8,128)(2,1)} async-done(((bf16[512,1536]{1,0:T(8,128)(2,1)}), bf16[2048,1536]{1,0:T(8,128)(2,1)}) %all-gather.12.cloned.1.call-update) | async-done | bytes 6291472 | tf_op jit(solution)/shard_map/all_gather | solution.py:83
  307.4 114.9 %all-gather.14.cloned.1.call-done = bf16[1536,2048]{1,0:T(8,128)(2,1)} async-done(((bf16[1536,512]{1,0:T(8,128)(2,1)}), bf16[1536,2048]{1,0:T(8,128)(2,1)}) %all-gather.14.cloned.1.call-update) | async-done | bytes 6291472 | tf_op jit(solution)/shard_map/all_gather | solution.py:94
  422.3 15.3 %convolution_convert_fusion = bf16[512,2048]{1,0:T(8,128)(2,1)} fusion(bf16[1536,2048]{1,0:T(8,128)(2,1)} %all-gather.14.cloned.1.call-done, bf16[512,1536]{1,0:T(8,128)(2,1)} %copy-done.4, bf16[1,1536]{1,0:T(2,128)(2,1)S(1)} %collective-permute-done.3, bf16[1,1536]{1,0:T(2,128)(2,1)S(1)} %collective-permute-done.2, f32[1536]{0:T(1024)S(1)} %get-tuple-element.8, ...), kind=kOutput, calls=%fused_computation.7 | convolution fusion | flops 6461587456 | bytes 18380800 | tf_op jit(solution)/shard_map/dot_general | solution.py:93
  437.6 29.5 %reduce-scatter.2.cloned.1.call-done = bf16[512,512]{1,0:T(8,128)(2,1)} async-done(((bf16[512,2048]{1,0:T(8,128)(2,1)}), bf16[512,512]{1,0:T(8,128)(2,1)}) %reduce-scatter.2.cloned.1.call-update) | async-done | bytes 524304 | tf_op jit(solution)/shard_map/reduce_scatter | solution.py:96
  467.1 2.0 add_convert_fusion
  (36 shorter events, 1.1 us)
Async XLA Ops:
  6.5 12.2 %copy-start = (bf16[512,256]{1,0:T(8,128)(2,1)S(1)}, bf16[512,256]{1,0:T(8,128)(2,1)}, u32[]{:S(2)}) copy-start(bf16[512,256]{1,0:T(8,128)(2,1)} %param.12) | copy-start | bytes 786436
  6.5 32.8 %all-gather.6.cloned.1.call-start = ((), (), s32[]{:S(2)}) async-start(), calls=%async_computation.1 | async-start | bytes 1310720 | tf_op jit(solution)/shard_map/all_gather | solution.py:63
  6.5 13.0 %copy-start.3 = (f32[2]{0:T(128)S(1)}, f32[2]{0:T(128)}, u32[]{:S(2)}) copy-start(f32[2]{0:T(128)} %param.15) | copy-start | bytes 28
  7.6 7.1 %collective-permute-start = (bf16[2,128,128]{2,1,0:T(8,128)(2,1)S(1)}, bf16[2,128,128]{2,1,0:T(8,128)(2,1)S(1)}, u32[]{:S(2)}, u32[]{:S(2)}) collective-permute-start(bf16[2,128,128]{2,1,0:T(8,128)(2,1)S(1)} %get-tuple-element.12), channel_id=1, source_target_pairs={{0,4},{4,8},{8,12},{1,5},{5,9},{9,13},{2,6},{6,10},{10,14},{3,7},{... | collective-permute-start | bytes 196616 | tf_op jit(solution)/shard_map/ppermute | solution.py:21
  12.6 6.2 %collective-permute-start.1 = (bf16[2,128,128]{2,1,0:T(8,128)(2,1)S(1)}, bf16[2,128,128]{2,1,0:T(8,128)(2,1)S(1)}, u32[]{:S(2)}, u32[]{:S(2)}) collective-permute-start(bf16[2,128,128]{2,1,0:T(8,128)(2,1)S(1)} %get-tuple-element.13), channel_id=1, source_target_pairs={{4,0},{8,4},{12,8},{5,1},{9,5},{13,9},{6,2},{10,6},{14,10},{7,3},{... | collective-permute-start | bytes 196616 | tf_op jit(solution)/shard_map/ppermute | solution.py:23
  22.3 53.2 %copy-start.5 = (bf16[512,2048]{1,0:T(8,128)(2,1)S(1)}, bf16[512,2048]{1,0:T(8,128)(2,1)}, u32[]{:S(2)}) copy-start(bf16[512,2048]{1,0:T(8,128)(2,1)} %param.16) | copy-start | bytes 6291460
  22.3 53.1 %all-gather.8.cloned.1.call-start = ((), (), s32[]{:S(2)}) async-start(), calls=%async_computation.2 | async-start | bytes 5242880 | tf_op jit(solution)/shard_map/all_gather | solution.py:66
  23.1 169.3 %all-gather.10.cloned.1.call-start = ((), (), s32[]{:S(2)}) async-start(), calls=%async_computation.3 | async-start | bytes 7864320 | tf_op jit(solution)/shard_map/all_gather | solution.py:78
  23.8 283.6 %all-gather.12.cloned.1.call-start = ((), (), s32[]{:S(2)}) async-start(), calls=%async_computation.4 | async-start | bytes 7864320 | tf_op jit(solution)/shard_map/all_gather | solution.py:83
  24.4 398.0 %all-gather.14.cloned.1.call-start = ((), (), s32[]{:S(2)}) async-start(), calls=%async_computation.5 | async-start | bytes 7864320 | tf_op jit(solution)/shard_map/all_gather | solution.py:94
  24.9 55.9 %copy-start.2 = (f32[2048]{0:T(1024)S(1)}, f32[2048]{0:T(1024)}, u32[]{:S(2)}) copy-start(f32[2048]{0:T(1024)} %param.18) | copy-start | bytes 24580
  25.0 442.2 %reduce-scatter.2.cloned.1.call-start = ((), (), s32[]{:S(2)}) async-start(), calls=%async_computation.6 | async-start | bytes 2621440 | tf_op jit(solution)/shard_map/reduce_scatter | solution.py:96
  81.5 119.9 %copy-start.1 = (f32[3,1536]{1,0:T(4,128)S(1)}, f32[3,1536]{1,0:T(4,128)}, u32[]{:S(2)}) copy-start(f32[3,1536]{1,0:T(4,128)} %param.21) | copy-start | bytes 55300
  81.5 340.9 %copy-start.6 = (f32[1536]{0:T(1024)S(1)}, f32[1536]{0:T(1024)}, u32[]{:S(2)}) copy-start(f32[1536]{0:T(1024)} %param.22) | copy-start | bytes 18436
  198.6 2.8 copy-start.4
  198.6 223.7 %collective-permute-start.2 = (bf16[1,1536]{1,0:T(2,128)(2,1)S(1)}, bf16[1,1536]{1,0:T(2,128)(2,1)S(1)}, u32[]{:S(2)}, u32[]{:S(2)}) collective-permute-start(bf16[1,1536]{1,0:T(2,128)(2,1)S(1)} %get-tuple-element.10), channel_id=1, source_target_pairs={{0,4},{4,8},{8,12},{1,5},{5,9},{9,13},{2,6},{6,10},{10,14},{3,7},{... | collective-permute-start | bytes 9224 | tf_op jit(solution)/shard_map/ppermute | solution.py:21
  199.9 222.4 %collective-permute-start.3 = (bf16[1,1536]{1,0:T(2,128)(2,1)S(1)}, bf16[1,1536]{1,0:T(2,128)(2,1)S(1)}, u32[]{:S(2)}, u32[]{:S(2)}) collective-permute-start(bf16[1,1536]{1,0:T(2,128)(2,1)S(1)} %get-tuple-element.11), channel_id=1, source_target_pairs={{4,0},{8,4},{12,8},{5,1},{9,5},{13,9},{6,2},{10,6},{14,10},{7,3},{... | collective-permute-start | bytes 9224 | tf_op jit(solution)/shard_map/ppermute | solution.py:23
Sparse Core Ops, SparseCore 0:
  22.4 16.9 all-gather.5
  40.9 34.4 all-gather.7
  77.0 115.3 all-gather.9
  193.8 113.5 all-gather.11
  308.8 113.4 all-gather.13
  437.7 29.3 reduce-scatter.1
where the time goes:
time: 476 us
  waiting for transfers between devices  418 us (88%)
  matrix products  29.4 us (6%)
  between operations  13.7 us (3%)
  starting transfers between devices  9.21 us (2%)
    all_gather x1, waiting for transfers between devices, shards(): lax.all_gather(w_down, 'sp', axis=1, tiled=True)  115 us
    all_gather x1, waiting for transfers between devices, shards(): lax.all_gather(w_gate, 'sp', axis=0, tiled=True)  111 us
    all_gather x1, waiting for transfers between devices, shards(): lax.all_gather(w_up, 'sp', axis=0, tiled=True)  106 us
    all_gather x1, waiting for transfers between devices, shards(): full_proj = lax.all_gather(out_proj, 'tp', axis=1, tiled=True)  36 us
    reduce_scatter x1, waiting for transfers between devices, shards(): lax.psum_scatter(terms.astype(jnp.bfloat16), 'tp', scatter_dimension=1, t...  29.5 us
    dot_general x1, matrix products, shards(): jnp.dot(act, lax.all_gather(w_down, 'sp', axis=1, tiled=True), preferred_...  15.3 us
    all_gather x1, waiting for transfers between devices, shards(): all_heads = lax.all_gather(heads_out, 'tp', axis=1, tiled=True)  14.4 us
  transfers between devices with their start and end apart: 10, of which 7 were waited for; matrix products, arithmetic and copies ran while one was open for 3% of the time, Pallas kernels for 0%

commit v1 on v0

v1 whole, which is shorter than its diff:
```python
import jax
import jax.numpy as jnp
from jax import lax
from jax.sharding import PartitionSpec as P


H = 8
KVH = 2
HD = 128
WINDOW = 128
CONV = 3
HALO = 16


def xor_pairs(count, mask):
    return [(i, i ^ mask) for i in range(count)]


def steps_of(levels):
    return sorted(range(1, levels), reverse=True)


def gather_tp(block):
    count = lax.axis_size("tp")
    slots = {0: block}
    mask = count // 2
    while mask:
        for j in sorted(slots):
            slots[j ^ mask] = lax.ppermute(slots[j], "tp", xor_pairs(count, mask))
        mask //= 2
    return slots


def attend(queries, keys, values, sink):
    tokens = queries.shape[0]
    heads_here = sink.shape[0]
    levels = lax.axis_size("sp")
    group = H // KVH
    scale = HD ** (-0.5)
    kv_head = (lax.axis_index("tp") * heads_here) // group
    own_keys = lax.dynamic_slice_in_dim(keys, kv_head * HD, HD, 1)
    own_values = lax.dynamic_slice_in_dim(values, kv_head * HD, HD, 1)
    both = jnp.stack([own_keys, own_values])
    up = [(i, i + 1) for i in range(levels - 1)]
    down = [(i + 1, i) for i in range(levels - 1)]
    before = lax.ppermute(both[:, tokens - WINDOW :], "sp", up)
    after = lax.ppermute(both[:, :WINDOW], "sp", down)
    extended = jnp.concatenate([before, both, after], axis=1)
    span = tokens + 2 * WINDOW
    q_heads = queries.reshape(tokens, heads_here, HD)
    scores = (
        jnp.einsum("qhd,kd->hqk", q_heads, extended[0], preferred_element_type=jnp.float32) * scale
    )
    offset = lax.axis_index("sp") * tokens
    q_pos = offset + jnp.arange(tokens, dtype=jnp.int32)[:, None]
    k_pos = offset - WINDOW + jnp.arange(span, dtype=jnp.int32)[None, :]
    valid = (jnp.abs(q_pos - k_pos) <= WINDOW) & (k_pos >= 0) & (k_pos < tokens * levels)
    scores = jnp.where(valid[None], scores, jnp.float32(-1e30))
    sink_col = sink[:, None]
    top = jnp.maximum(jnp.max(scores, axis=-1), sink_col)
    expo = jnp.exp(scores - top[..., None])
    total = jnp.sum(expo, axis=-1) + jnp.exp(sink_col - top)
    weights = (expo / total[..., None]).astype(jnp.bfloat16)
    mixed = jnp.einsum("hqk,kd->qhd", weights, extended[1], preferred_element_type=jnp.float32)
    return mixed.astype(jnp.bfloat16).reshape(tokens, heads_here * HD)


def layer(
    queries, keys, values, sink, resid, out_proj, norm_gain, w_gate, w_up, conv_w, conv_b, w_down
):
    tokens = queries.shape[0]
    width = resid.shape[1]
    levels = lax.axis_size("sp")
    count = lax.axis_size("tp")
    level = lax.axis_index("sp")
    tp = lax.axis_index("tp")
    part = lax.axis_index("grp")
    odd = level & 1
    cols = width // count
    rows_lv = width // levels
    hidden = w_gate.shape[1]
    half = hidden // 2

    def gu_piece(dest_odd, share):
        rows = rows_lv // 2
        return jnp.concatenate(
            [
                lax.dynamic_slice(w, (share * rows, dest_odd * half), (rows, half))
                for w in (w_gate, w_up)
            ],
            axis=1,
        )

    def d_piece(dest_odd, share):
        rows = half // 2
        return lax.dynamic_slice(w_down, (dest_odd * half + share * rows, 0), (rows, rows_lv))

    swap = [(0, 1), (1, 0)]
    gu_full = jnp.zeros((width, 2 * half), w_gate.dtype)
    d_full = jnp.zeros((half, width), w_down.dtype)

    def put_gu(full, piece, source, share):
        return lax.dynamic_update_slice(
            full, piece, (source * rows_lv + share * (rows_lv // 2), 0)
        )

    def put_d(full, piece, source, share):
        start = source * rows_lv
        slot = (start // cols) ^ tp
        place = (slot >> 1) + (slot & 1) * (count // 2)
        return lax.dynamic_update_slice(
            full, piece, (share * (half // 2), place * cols + start % cols)
        )

    for share in range(2):
        gu_full = put_gu(gu_full, gu_piece(odd, share), level, share)
        d_full = put_d(d_full, d_piece(odd, share), level, share)
    for mask in steps_of(levels):
        got = lax.ppermute(gu_piece(odd ^ (mask & 1), part), "sp", xor_pairs(levels, mask))
        other = lax.ppermute(got, "grp", swap)
        gu_full = put_gu(gu_full, got, level ^ mask, part)
        gu_full = put_gu(gu_full, other, level ^ mask, 1 - part)
    for mask in steps_of(levels):
        got = lax.ppermute(d_piece(odd ^ (mask & 1), part), "sp", xor_pairs(levels, mask))
        other = lax.ppermute(got, "grp", swap)
        d_full = put_d(d_full, got, level ^ mask, part)
        d_full = put_d(d_full, other, level ^ mask, 1 - part)

    mixed = attend(queries, keys, values, sink)
    head_cols = mixed.shape[1]
    all_heads = jnp.zeros((tokens, count * head_cols), mixed.dtype)
    for j, block in gather_tp(mixed).items():
        all_heads = lax.dynamic_update_slice(all_heads, block, (0, (tp ^ j) * head_cols))
    resid_own = lax.dynamic_slice_in_dim(resid, tp * cols, cols, 1)
    gain_own = lax.dynamic_slice_in_dim(norm_gain, tp * cols, cols, 0)
    summed = resid_own.astype(jnp.float32) + jnp.dot(
        all_heads, out_proj, preferred_element_type=jnp.float32
    )
    sums = jnp.stack([jnp.sum(summed, axis=-1), jnp.sum(summed * summed, axis=-1)])
    totals = sums
    for j in range(1, count):
        totals = totals + lax.ppermute(sums, "tp", xor_pairs(count, j))
    mean = (totals[0] / width)[:, None]
    msq = (totals[1] / width)[:, None]
    normed = ((summed - mean) * lax.rsqrt(msq - mean * mean + 1e-05) * gain_own).astype(
        jnp.bfloat16
    )

    outer = jnp.where(odd == 1, normed[tokens - HALO :], normed[:HALO])
    near = [(i, i + 1 if i & 1 else i - 1) for i in range(levels)]
    far = [(i, i + 2 if i & 1 else i - 2) for i in range(levels)]
    near = [(a, b) for a, b in near if 0 <= b < levels]
    far = [(a, b) for a, b in far if 0 <= b < levels]
    rows = 2 * tokens + 2 * HALO
    last = rows - HALO
    mate = lax.ppermute(normed, "sp", xor_pairs(levels, 1))
    edge_a = lax.ppermute(outer, "sp", near)
    edge_b = lax.ppermute(outer, "sp", far)
    pair = jnp.zeros((rows, cols), normed.dtype)
    pair = lax.dynamic_update_slice(pair, normed, (HALO + odd * tokens, 0))
    pair = lax.dynamic_update_slice(pair, mate, (HALO + (1 - odd) * tokens, 0))
    pair = lax.dynamic_update_slice(pair, edge_a, (odd * last, 0))
    pair = lax.dynamic_update_slice(pair, edge_b, ((1 - odd) * last, 0))
    normed_all = jnp.zeros((rows, width), normed.dtype)
    for j, block in gather_tp(pair).items():
        normed_all = lax.dynamic_update_slice(normed_all, block, (0, (tp ^ j) * cols))

    both = jnp.dot(normed_all, gu_full, preferred_element_type=jnp.float32).astype(jnp.bfloat16)
    taps = lax.dynamic_slice_in_dim(conv_w, odd * half, half, 1)
    conv = lax.dynamic_slice_in_dim(conv_b, odd * half, half, 0)
    first = HALO - CONV // 2
    for tap in range(CONV):
        gate = both[first + tap : first + tap + 2 * tokens, :half]
        conv = conv + gate.astype(jnp.float32) * taps[tap]
    up_part = both[HALO : HALO + 2 * tokens, half:]
    act = (jax.nn.silu(conv) * up_part.astype(jnp.float32)).astype(jnp.bfloat16)
    mine = width // 2
    away = jnp.dot(act, d_full[:, mine:], preferred_element_type=jnp.float32).astype(jnp.bfloat16)
    came = lax.ppermute(away, "tp", xor_pairs(count, 1))
    here = jnp.dot(act, d_full[:, :mine], preferred_element_type=jnp.float32)
    here = here + came.astype(jnp.float32)

    def block_of(step, slot):
        start = (odd ^ step) * tokens
        return lax.dynamic_slice(here, (start, slot * cols), (tokens, cols))

    ffn = block_of(0, 0)
    for step in range(2):
        for slot in range(count // 2):
            if step or slot:
                pairs = [
                    (i * count + j, (i ^ step) * count + (j ^ (2 * slot)))
                    for i in range(levels)
                    for j in range(count)
                ]
                ffn = ffn + lax.ppermute(
                    block_of(step, slot).astype(jnp.bfloat16), ("sp", "tp"), pairs
                ).astype(jnp.float32)
    return (normed.astype(jnp.float32) + ffn).astype(jnp.bfloat16)


def solution(mesh):
    return jax.shard_map(
        layer,
        mesh=mesh,
        in_specs=(
            P(("grp", "sp"), "tp"),
            P(("grp", "sp"), None),
            P(("grp", "sp"), None),
            P("tp"),
            P(("grp", "sp"), None),
            P(None, "tp"),
            P(),
            P("sp", "tp"),
            P("sp", "tp"),
            P(None, "tp"),
            P("tp"),
            P("tp", "sp"),
        ),
        out_specs=P(("grp", "sp"), "tp"),
        check_vma=False,
    )
```

time: 476 us -> 266 us (0.56)
  waiting for transfers between devices: 418 us -> 106 us
  local copies, waits for them, and re-layouts: 1.13 us -> 59.6 us
  starting transfers between devices: 9.21 us -> 64.3 us
  between operations: 13.7 us -> 0.4 us
  other arithmetic: 4.34 us -> 11.4 us
  matrix products: 29.4 us -> 22.8 us
    all_gather x5 -> x0, waiting for transfers between devices: 382 us -> none  [the longest x1 115 us: shards(): lax.all_gather(w_down, 'sp', axis=1, tiled=True)]
    ppermute x4 -> x30, waiting for transfers between devices: 4.03 us -> 106 us  [the longest x3 47.4 us: layer(): lax.ppermute(d_piece(odd ^ mask & 1, part), 'sp', xor_pairs(levels, mask))]
    ppermute x4 -> x30, starting transfers between devices: 9.01 us -> 64.3 us  [the longest x3 21.6 us: layer(): lax.ppermute(gu_piece(odd ^ mask & 1, part), 'sp', xor_pairs(levels, mask))]
    dynamic_update_slice x0 -> x24, local copies, waits for them, and re-layouts: none -> 46.5 us  [the longest x7 32.2 us: put_d(): lax.dynamic_update_slice(full, piece, (share * (half // 2), place * cols...]
    reduce_scatter x1 -> x0, waiting for transfers between devices: 29.5 us -> none  [shards(): lax.psum_scatter(terms.astype(jnp.bfloat16), 'tp', scatter_dimension=1, t...]
    dot_general x5 -> x6, matrix products: 29.4 us -> 22.8 us  [the longest x1 9 us: layer(): jnp.dot(normed_all, gu_full, preferred_element_type=jnp.float32)]
    broadcast_in_dim x0 -> x5, local copies, waits for them, and re-layouts: none -> 5.82 us  [the longest x1 3.04 us: layer(): gu_full = jnp.zeros((width, 2 * half), w_gate.dtype)]
    dynamic_slice x0 -> x4, local copies, waits for them, and re-layouts: none -> 5.1 us  [the longest x1 3.17 us: gu_piece(): lax.dynamic_slice(w, (share * rows, dest_odd * half), (rows, half))]
  transfers between devices with their start and end apart: 10 -> 30, of which waited for: 7 -> 12; matrix products, arithmetic and copies ran while one was open for 3% -> 26% of each run, Pallas kernels for 0% -> 0%
where the time goes in v1:
time: 266 us; the launch traced here: 265 us
  waiting for transfers between devices  106 us (40%)
  starting transfers between devices  64.3 us (24%)
  local copies, waits for them, and re-layouts  59.6 us (22%)
  matrix products  22.8 us (9%)
  other arithmetic  11.4 us (4%)
    ppermute x3, waiting for transfers between devices, layer(): lax.ppermute(d_piece(odd ^ mask & 1, part), 'sp', xor_pairs(levels, mask))  47.4 us
    dynamic_update_slice x7, local copies, waits for them, and re-layouts, put_d(): lax.dynamic_update_slice(full, piece, (share * (half // 2), place * cols...  32.2 us
    ppermute x6, waiting for transfers between devices, layer(): other = lax.ppermute(got, 'grp', swap)  26.5 us
    ppermute x3, waiting for transfers between devices, layer(): lax.ppermute(block_of(step, slot).astype(jnp.bfloat16), ('sp', 'tp'), pairs)  22.9 us
    ppermute x3, starting transfers between devices, layer(): lax.ppermute(gu_piece(odd ^ mask & 1, part), 'sp', xor_pairs(levels, mask))  21.6 us
    ppermute x3, starting transfers between devices, layer(): lax.ppermute(d_piece(odd ^ mask & 1, part), 'sp', xor_pairs(levels, mask))  19.6 us
    dynamic_update_slice x6, local copies, waits for them, and re-layouts, put_gu(): lax.dynamic_update_slice(full, piece, (source * rows_lv + share * (rows_l...  10.2 us
    dot_general x1, matrix products, layer(): jnp.dot(normed_all, gu_full, preferred_element_type=jnp.float32)  9 us
  transfers between devices with their start and end apart: 30, of which 12 were waited for; matrix products, arithmetic and copies ran while one was open for 26% of the time, Pallas kernels for 0%

profile of v1, /device:TPU:0, one launch (start us, length us, event | category | flops | bytes accessed | tf_op | source)
XLA Modules:
  0.0 264.7 jit_solution(13357013502735301259)
XLA Ops:
  1.1 5.0 %collective-permute-start = (bf16[2,128,128]{2,1,0:T(8,128)(2,1)S(1)}, bf16[2,128,128]{2,1,0:T(8,128)(2,1)S(1)}, u32[]{:S(2)}, u32[]{:S(2)}) collective-permute-start(bf16[2,128,128]{2,1,0:T(8,128)(2,1)S(1)} %get-tuple-element.26), channel_id=1, source_target_pairs={{0,4},{4,8},{8,12},{1,5},{5,9},{9,13},{2,6},{6,10},{10,14},{3,7},{... | collective-permute-start | bytes 196616 | tf_op jit(solution)/shard_map/ppermute | solution.py:46
  8.2 3.2 %fusion.17 = (bf16[256,768]{1,0:T(8,128)(2,1)}, bf16[256,768]{1,0:T(8,128)(2,1)S(1)}, bf16[256,768]{1,0:T(8,128)(2,1)}, bf16[256,768]{1,0:T(8,128)(2,1)S(1)}, bf...) fusion(bf16[512,1536]{1,0:T(8,128)(2,1)} %param.19, ...), kind=kLoop, calls=%fused_computation.82 | loop fusion | bytes 6291468 | tf_op jit(solution)/shard_map/dynamic_slice | solution.py:88
  18.3 3.9 %collective-permute-start.14 = (bf16[256,1536]{1,0:T(8,128)(2,1)}, bf16[256,1536]{1,0:T(8,128)(2,1)}, u32[]{:S(2)}, u32[]{:S(2)}) collective-permute-start(bf16[256,1536]{1,0:T(8,128)(2,1)} %pad_maximum_fusion), channel_id=1, source_target_pairs={{0,12},{4,8},{8,4},{12,0},{1,13},{5,9},{9,5},{13,1},{2,14},{6,10},... | collective-permute-start | bytes 2359304 | tf_op jit(solution)/shard_map/ppermute | solution.py:119
  41.5 24.8 %collective-permute-done.20 = bf16[384,512]{1,0:T(8,128)(2,1)} collective-permute-done((bf16[384,512]{1,0:T(8,128)(2,1)}, bf16[384,512]{1,0:T(8,128)(2,1)}, u32[]{:S(2)}, u32[]{:S(2)}) %collective-permute-start.20) | collective-permute-done | bytes 393248 | tf_op jit(solution)/shard_map/ppermute | solution.py:124
  66.3 17.7 %collective-permute-start.16 = (bf16[256,1536]{1,0:T(8,128)(2,1)}, bf16[256,1536]{1,0:T(8,128)(2,1)}, u32[]{:S(2)}, u32[]{:S(2)}) collective-permute-start(bf16[256,1536]{1,0:T(8,128)(2,1)} %pad_maximum_fusion.1), channel_id=1, source_target_pairs={{0,8},{4,12},{8,0},{12,4},{1,9},{5,13},{9,1},{13,5},{2,10},{6,14},... | collective-permute-start | bytes 2359304 | tf_op jit(solution)/shard_map/ppermute | solution.py:119
  84.0 22.6 %collective-permute-done.22 = bf16[384,512]{1,0:T(8,128)(2,1)S(1)} collective-permute-done((bf16[384,512]{1,0:T(8,128)(2,1)}, bf16[384,512]{1,0:T(8,128)(2,1)S(1)}, u32[]{:S(2)}, u32[]{:S(2)}) %collective-permute-start.22) | collective-permute-done | bytes 393248 | tf_op jit(solution)/shard_map/ppermute | solution.py:124
  107.3 16.2 %collective-permute-start.24 = (bf16[384,512]{1,0:T(8,128)(2,1)}, bf16[384,512]{1,0:T(8,128)(2,1)}, u32[]{:S(2)}, u32[]{:S(2)}) collective-permute-start(bf16[384,512]{1,0:T(8,128)(2,1)} %get-tuple-element.17), channel_id=1, source_target_pairs={{0,4},{4,0},{8,12},{12,8},{1,5},{5,1},{9,13},{13,9},{2,6},{6,2},{1... | collective-permute-start | bytes 1179656 | tf_op jit(solution)/shard_map/ppermute | solution.py:124
  123.4 3.0 %broadcast_in_dim.42 = bf16[2048,1536]{1,0:T(8,128)(2,1)} broadcast(bf16[]{:T(256)} %constant.128.clone.1), dimensions={} | broadcast | bytes 6291458 | tf_op jit(solution)/shard_map/broadcast_in_dim | solution.py:99
  130.0 4.0 %collective-permute-done.10 = bf16[16,512]{1,0:T(8,128)(2,1)S(1)} collective-permute-done((bf16[16,512]{1,0:T(8,128)(2,1)S(1)}, bf16[16,512]{1,0:T(8,128)(2,1)S(1)}, u32[]{:S(2)}, u32[]{:S(2)}) %collective-permute-start.10) | collective-permute-done | bytes 16416 | tf_op jit(solution)/shard_map/ppermute | solution.py:158
  140.6 5.2 %dynamic_update_slice.106 = bf16[768,2048]{1,0:T(8,128)(2,1)} dynamic-update-slice(bf16[768,2048]{1,0:T(8,128)(2,1)} %get-tuple-element.16, bf16[384,512]{1,0:T(8,128)(2,1)} %collective-permute-done.20, s32[]{:T(128)S(6)} %select_n.227, s32[]{:T(128)S(6)} %select_n.230) | dynamic-update-slice | bytes 786436 | tf_op jit(solution)/shard_map/dynamic_update_slice | solution.py:111
  149.8 4.9 %dynamic_update_slice.107 = bf16[768,2048]{1,0:T(8,128)(2,1)} dynamic-update-slice(bf16[768,2048]{1,0:T(8,128)(2,1)} %dynamic_update_slice.106, bf16[384,512]{1,0:T(8,128)(2,1)} %collective-permute-done.21, s32[]{:T(128)S(6)} %select_n.231, s32[]{:T(128)S(6)} %select_n.230) | dynamic-update-slice | bytes 786436 | tf_op jit(solution)/shard_map/dynamic_update_slice | solution.py:111
  154.7 5.6 %dynamic_update_slice.108 = bf16[768,2048]{1,0:T(8,128)(2,1)} dynamic-update-slice(bf16[768,2048]{1,0:T(8,128)(2,1)} %dynamic_update_slice.107, bf16[384,512]{1,0:T(8,128)(2,1)S(1)} %copy-done.6, s32[]{:T(128)S(6)} %select_n.227, s32[]{:T(128)S(6)} %select_n.235) | dynamic-update-slice | bytes 786436 | tf_op jit(solution)/shard_map/dynamic_update_slice | solution.py:111
  160.3 4.9 %dynamic_update_slice.109 = bf16[768,2048]{1,0:T(8,128)(2,1)} dynamic-update-slice(bf16[768,2048]{1,0:T(8,128)(2,1)} %dynamic_update_slice.108, bf16[384,512]{1,0:T(8,128)(2,1)} %collective-permute-done.23, s32[]{:T(128)S(6)} %select_n.231, s32[]{:T(128)S(6)} %select_n.235) | dynamic-update-slice | bytes 786436 | tf_op jit(solution)/shard_map/dynamic_update_slice | solution.py:111
  165.2 5.9 %dynamic_update_slice.110 = bf16[768,2048]{1,0:T(8,128)(2,1)} dynamic-update-slice(bf16[768,2048]{1,0:T(8,128)(2,1)} %dynamic_update_slice.109, bf16[384,512]{1,0:T(8,128)(2,1)} %collective-permute-done.24, s32[]{:T(128)S(6)} %select_n.227, s32[]{:T(128)S(6)} %select_n.238) | dynamic-update-slice | bytes 786436 | tf_op jit(solution)/shard_map/dynamic_update_slice | solution.py:111
  171.1 5.0 %dynamic_update_slice.111 = bf16[768,2048]{1,0:T(8,128)(2,1)} dynamic-update-slice(bf16[768,2048]{1,0:T(8,128)(2,1)} %dynamic_update_slice.110, bf16[384,512]{1,0:T(8,128)(2,1)} %collective-permute-done.25, s32[]{:T(128)S(6)} %select_n.231, s32[]{:T(128)S(6)} %select_n.238) | dynamic-update-slice | bytes 786436 | tf_op jit(solution)/shard_map/dynamic_update_slice | solution.py:111
  176.9 3.1 %collective-permute-done.15 = bf16[256,1536]{1,0:T(8,128)(2,1)} collective-permute-done((bf16[256,1536]{1,0:T(8,128)(2,1)}, bf16[256,1536]{1,0:T(8,128)(2,1)}, u32[]{:S(2)}, u32[]{:S(2)}) %collective-permute-start.15) | collective-permute-done | bytes 786464 | tf_op jit(solution)/shard_map/ppermute | solution.py:120
  184.1 12.6 %collective-permute-done.17 = bf16[256,1536]{1,0:T(8,128)(2,1)S(1)} collective-permute-done((bf16[256,1536]{1,0:T(8,128)(2,1)}, bf16[256,1536]{1,0:T(8,128)(2,1)S(1)}, u32[]{:S(2)}, u32[]{:S(2)}) %collective-permute-start.17) | collective-permute-done | bytes 786464 | tf_op jit(solution)/shard_map/ppermute | solution.py:120
  199.7 10.4 %collective-permute-done.19 = bf16[256,1536]{1,0:T(8,128)(2,1)S(1)} collective-permute-done((bf16[256,1536]{1,0:T(8,128)(2,1)}, bf16[256,1536]{1,0:T(8,128)(2,1)S(1)}, u32[]{:S(2)}, u32[]{:S(2)}) %collective-permute-start.19) | collective-permute-done | bytes 786464 | tf_op jit(solution)/shard_map/ppermute | solution.py:120
  212.8 9.0 %convolution_convert_fusion = bf16[1056,1536]{1,0:T(8,128)(2,1)S(1)} fusion(bf16[1056,2048]{1,0:T(8,128)(2,1)S(1)} %constant_dynamic-update-slice_fusion.6, bf16[2048,1536]{1,0:T(8,128)(2,1)} %constant_dynamic-update-slice_fusion), kind=kOutput, calls=%fused_computation | convolution fusion | flops 6645399552 | bytes 13860864 | tf_op jit(solution)/shard_map/dot_general | solution.py:168
  223.9 4.5 %convolution_convert_fusion.1 = bf16[1024,1024]{1,0:T(8,128)(2,1)} fusion(bf16[1024,768]{1,0:T(8,128)(2,1)S(1)} %multiply_convert_fusion, bf16[768,2048]{1,0:T(8,128)(2,1)} %dynamic_update_slice.111), kind=kOutput, calls=%fused_computation.8 | convolution fusion | flops 1611661312 | bytes 5242880 | tf_op jit(solution)/shard_map/dot_general | solution.py:178
  228.4 4.5 %collective-permute-done.26 = bf16[1024,1024]{1,0:T(8,128)(2,1)} collective-permute-done((bf16[1024,1024]{1,0:T(8,128)(2,1)}, bf16[1024,1024]{1,0:T(8,128)(2,1)}, u32[]{:S(2)}, u32[]{:S(2)}) %collective-permute-start.26) | collective-permute-done | bytes 2097184 | tf_op jit(solution)/shard_map/ppermute | solution.py:179
  232.9 3.9 %convert_add_fusion = f32[1024,1024]{1,0:T(8,128)S(1)} fusion(bf16[1024,1024]{1,0:T(8,128)(2,1)} %collective-permute-done.26, bf16[1024,768]{1,0:T(8,128)(2,1)S(1)} %multiply_convert_fusion, bf16[768,2048]{1,0:T(8,128)(2,1)} %dynamic_update_slice.111), kind=kOutput, calls=%fused_computation.1 | convolution fusion | flops 1612709888 | bytes 9437184 | tf_op jit(solution)/shard_map/dot_general | solution.py:180
  240.6 10.5 %collective-permute-done.27 = bf16[512,512]{1,0:T(8,128)(2,1)S(1)} collective-permute-done((bf16[512,512]{1,0:T(8,128)(2,1)S(1)}, bf16[512,512]{1,0:T(8,128)(2,1)S(1)}, u32[]{:S(2)}, u32[]{:S(2)}) %collective-permute-start.27) | collective-permute-done | bytes 524320 | tf_op jit(solution)/shard_map/ppermute | solution.py:196
  252.4 11.1 %collective-permute-done.29 = bf16[512,512]{1,0:T(8,128)(2,1)S(1)} collective-permute-done((bf16[512,512]{1,0:T(8,128)(2,1)S(1)}, bf16[512,512]{1,0:T(8,128)(2,1)S(1)}, u32[]{:S(2)}, u32[]{:S(2)}) %collective-permute-start.29) | collective-permute-done | bytes 524320 | tf_op jit(solution)/shard_map/ppermute | solution.py:196
  (119 shorter events, 63.1 us)
Async XLA Ops:
  1.1 10.3 %collective-permute-start = (bf16[2,128,128]{2,1,0:T(8,128)(2,1)S(1)}, bf16[2,128,128]{2,1,0:T(8,128)(2,1)S(1)}, u32[]{:S(2)}, u32[]{:S(2)}) collective-permute-start(bf16[2,128,128]{2,1,0:T(8,128)(2,1)S(1)} %get-tuple-element.26), channel_id=1, source_target_pairs={{0,4},{4,8},{8,12},{1,5},{5,9},{9,13},{2,6},{6,10},{10,14},{3,7},{... | collective-permute-start | bytes 196616 | tf_op jit(solution)/shard_map/ppermute | solution.py:46
  6.1 6.2 %collective-permute-start.1 = (bf16[2,128,128]{2,1,0:T(8,128)(2,1)S(1)}, bf16[2,128,128]{2,1,0:T(8,128)(2,1)S(1)}, u32[]{:S(2)}, u32[]{:S(2)}) collective-permute-start(bf16[2,128,128]{2,1,0:T(8,128)(2,1)S(1)} %get-tuple-element.27), channel_id=1, source_target_pairs={{4,0},{8,4},{12,8},{5,1},{9,5},{13,9},{6,2},{10,6},{14,10},{7,3},{... | collective-permute-start | bytes 196616 | tf_op jit(solution)/shard_map/ppermute | solution.py:47
  15.8 9.2 %collective-permute-start.2 = (bf16[512,256]{0,1:T(8,128)(2,1)}, bf16[512,256]{0,1:T(8,128)(2,1)S(1)}, u32[]{:S(2)}, u32[]{:S(2)}) collective-permute-start(bf16[512,256]{0,1:T(8,128)(2,1)} %bitcast.8), channel_id=1, source_target_pairs={{0,2},{1,3},{2,0},{3,1},{4,6},{5,7},{6,4},{7,5},{8,10},{9,11},{10,... | collective-permute-start | bytes 786440 | tf_op jit(solution)/shard_map/ppermute | solution.py:29
  18.3 117.8 %collective-permute-start.14 = (bf16[256,1536]{1,0:T(8,128)(2,1)}, bf16[256,1536]{1,0:T(8,128)(2,1)}, u32[]{:S(2)}, u32[]{:S(2)}) collective-permute-start(bf16[256,1536]{1,0:T(8,128)(2,1)} %pad_maximum_fusion), channel_id=1, source_target_pairs={{0,12},{4,8},{8,4},{12,0},{1,13},{5,9},{9,5},{13,1},{2,14},{6,10},... | collective-permute-start | bytes 2359304 | tf_op jit(solution)/shard_map/ppermute | solution.py:119
  22.2 115.9 %collective-permute-start.18 = (bf16[256,1536]{1,0:T(8,128)(2,1)}, bf16[256,1536]{1,0:T(8,128)(2,1)}, u32[]{:S(2)}, u32[]{:S(2)}) collective-permute-start(bf16[256,1536]{1,0:T(8,128)(2,1)} %pad_maximum_fusion), channel_id=1, source_target_pairs={{0,4},{4,0},{8,12},{12,8},{1,5},{5,1},{9,13},{13,9},{2,6},{6,2},{1... | collective-permute-start | bytes 2359304 | tf_op jit(solution)/shard_map/ppermute | solution.py:119
  30.6 6.3 %collective-permute-start.7 = (f32[2,512]{1,0:T(2,128)S(1)}, f32[2,512]{1,0:T(2,128)S(1)}, u32[]{:S(2)}, u32[]{:S(2)}) collective-permute-start(f32[2,512]{1,0:T(2,128)S(1)} %pad_maximum_fusion.5), channel_id=1, source_target_pairs={{0,3},{1,2},{2,1},{3,0},{4,7},{5,6},{6,5},{7,4},{8,11},{9,10},{10,... | collective-permute-start | bytes 12296 | tf_op jit(solution)/shard_map/ppermute | solution.py:142
  33.4 32.9 %collective-permute-start.20 = (bf16[384,512]{1,0:T(8,128)(2,1)}, bf16[384,512]{1,0:T(8,128)(2,1)}, u32[]{:S(2)}, u32[]{:S(2)}) collective-permute-start(bf16[384,512]{1,0:T(8,128)(2,1)} %get-tuple-element.17), channel_id=1, source_target_pairs={{0,12},{4,8},{8,4},{12,0},{1,13},{5,9},{9,5},{13,1},{2,14},{6,10},... | collective-permute-start | bytes 1179656 | tf_op jit(solution)/shard_map/ppermute | solution.py:124
  35.6 71.0 %collective-permute-start.22 = (bf16[384,512]{1,0:T(8,128)(2,1)}, bf16[384,512]{1,0:T(8,128)(2,1)S(1)}, u32[]{:S(2)}, u32[]{:S(2)}) collective-permute-start(bf16[384,512]{1,0:T(8,128)(2,1)} %get-tuple-element.15), channel_id=1, source_target_pairs={{0,8},{4,12},{8,0},{12,4},{1,9},{5,13},{9,1},{13,5},{2,10},{6,14},... | collective-permute-start | bytes 1179656 | tf_op jit(solution)/shard_map/ppermute | solution.py:124
  38.5 88.9 %collective-permute-start.8 = (bf16[512,512]{1,0:T(8,128)(2,1)S(1)}, bf16[512,512]{1,0:T(8,128)(2,1)}, u32[]{:S(2)}, u32[]{:S(2)}) collective-permute-start(bf16[512,512]{1,0:T(8,128)(2,1)S(1)} %get-tuple-element.11), channel_id=1, source_target_pairs={{0,4},{4,0},{8,12},{12,8},{1,5},{5,1},{9,13},{13,9},{2,6},{6,2},{1... | collective-permute-start | bytes 1572872 | tf_op jit(solution)/shard_map/ppermute | solution.py:156
  66.3 71.2 %collective-permute-start.16 = (bf16[256,1536]{1,0:T(8,128)(2,1)}, bf16[256,1536]{1,0:T(8,128)(2,1)}, u32[]{:S(2)}, u32[]{:S(2)}) collective-permute-start(bf16[256,1536]{1,0:T(8,128)(2,1)} %pad_maximum_fusion.1), channel_id=1, source_target_pairs={{0,8},{4,12},{8,0},{12,4},{1,9},{5,13},{9,1},{13,5},{2,10},{6,14},... | collective-permute-start | bytes 2359304 | tf_op jit(solution)/shard_map/ppermute | solution.py:119
  107.3 28.2 %collective-permute-start.24 = (bf16[384,512]{1,0:T(8,128)(2,1)}, bf16[384,512]{1,0:T(8,128)(2,1)}, u32[]{:S(2)}, u32[]{:S(2)}) collective-permute-start(bf16[384,512]{1,0:T(8,128)(2,1)} %get-tuple-element.17), channel_id=1, source_target_pairs={{0,4},{4,0},{8,12},{12,8},{1,5},{5,1},{9,13},{13,9},{2,6},{6,2},{1... | collective-permute-start | bytes 1179656 | tf_op jit(solution)/shard_map/ppermute | solution.py:124
  127.4 6.5 %collective-permute-start.10 = (bf16[16,512]{1,0:T(8,128)(2,1)S(1)}, bf16[16,512]{1,0:T(8,128)(2,1)S(1)}, u32[]{:S(2)}, u32[]{:S(2)}) collective-permute-start(bf16[16,512]{1,0:T(8,128)(2,1)S(1)} %slice_select_fusion), channel_id=1, source_target_pairs={{4,12},{8,0},{5,13},{9,1},{6,14},{10,2},{7,15},{11,3},{20,28},{24,... | collective-permute-start | bytes 49160 | tf_op jit(solution)/shard_map/ppermute | solution.py:158
  134.0 12.3 %collective-permute-start.21 = (bf16[384,512]{1,0:T(8,128)(2,1)}, bf16[384,512]{1,0:T(8,128)(2,1)}, u32[]{:S(2)}, u32[]{:S(2)}) collective-permute-start(bf16[384,512]{1,0:T(8,128)(2,1)} %collective-permute-done.20), channel_id=1, source_target_pairs={{0,16},{16,0},{1,17},{17,1},{2,18},{18,2},{3,19},{19,3},{4,20},{20... | collective-permute-start | bytes 1179656 | tf_op jit(solution)/shard_map/ppermute | solution.py:125
  135.4 24.9 %collective-permute-start.23 = (bf16[384,512]{1,0:T(8,128)(2,1)}, bf16[384,512]{1,0:T(8,128)(2,1)}, u32[]{:S(2)}, u32[]{:S(2)}) collective-permute-start(bf16[384,512]{1,0:T(8,128)(2,1)} %copy-done.5), channel_id=1, source_target_pairs={{0,16},{16,0},{1,17},{17,1},{2,18},{18,2},{3,19},{19,3},{4,20},{20... | collective-permute-start | bytes 1179656 | tf_op jit(solution)/shard_map/ppermute | solution.py:125
  136.1 35.1 %collective-permute-start.25 = (bf16[384,512]{1,0:T(8,128)(2,1)}, bf16[384,512]{1,0:T(8,128)(2,1)}, u32[]{:S(2)}, u32[]{:S(2)}) collective-permute-start(bf16[384,512]{1,0:T(8,128)(2,1)} %collective-permute-done.24), channel_id=1, source_target_pairs={{0,16},{16,0},{1,17},{17,1},{2,18},{18,2},{3,19},{19,3},{4,20},{20... | collective-permute-start | bytes 1179656 | tf_op jit(solution)/shard_map/ppermute | solution.py:125
  137.5 42.4 %collective-permute-start.15 = (bf16[256,1536]{1,0:T(8,128)(2,1)}, bf16[256,1536]{1,0:T(8,128)(2,1)}, u32[]{:S(2)}, u32[]{:S(2)}) collective-permute-start(bf16[256,1536]{1,0:T(8,128)(2,1)} %collective-permute-done.14), channel_id=1, source_target_pairs={{0,16},{16,0},{1,17},{17,1},{2,18},{18,2},{3,19},{19,3},{4,20},{20... | collective-permute-start | bytes 2359304 | tf_op jit(solution)/shard_map/ppermute | solution.py:120
  138.1 46.0 %collective-permute-start.11 = (bf16[1056,512]{1,0:T(8,128)(2,1)S(1)}, bf16[1056,512]{1,0:T(8,128)(2,1)}, u32[]{:S(2)}, u32[]{:S(2)}) collective-permute-start(bf16[1056,512]{1,0:T(8,128)(2,1)S(1)} %constant_dynamic-update-slice_fusion.10), channel_id=1, source_target_pairs={{0,2},{1,3},{2,0},{3,1},{4,6},{5,7},{6,4},{7,5},{8,10},{9,11},{10,... | collective-permute-start | bytes 3244040 | tf_op jit(solution)/shard_map/ppermute | solution.py:29
  146.3 50.5 %collective-permute-start.17 = (bf16[256,1536]{1,0:T(8,128)(2,1)}, bf16[256,1536]{1,0:T(8,128)(2,1)S(1)}, u32[]{:S(2)}, u32[]{:S(2)}) collective-permute-start(bf16[256,1536]{1,0:T(8,128)(2,1)} %collective-permute-done.16), channel_id=1, source_target_pairs={{0,16},{16,0},{1,17},{17,1},{2,18},{18,2},{3,19},{19,3},{4,20},{20... | collective-permute-start | bytes 2359304 | tf_op jit(solution)/shard_map/ppermute | solution.py:120
  160.3 49.8 %collective-permute-start.19 = (bf16[256,1536]{1,0:T(8,128)(2,1)}, bf16[256,1536]{1,0:T(8,128)(2,1)S(1)}, u32[]{:S(2)}, u32[]{:S(2)}) collective-permute-start(bf16[256,1536]{1,0:T(8,128)(2,1)} %collective-permute-done.18), channel_id=1, source_target_pairs={{0,16},{16,0},{1,17},{17,1},{2,18},{18,2},{3,19},{19,3},{4,20},{20... | collective-permute-start | bytes 2359304 | tf_op jit(solution)/shard_map/ppermute | solution.py:120
  176.1 36.4 %collective-permute-start.12 = (bf16[1056,512]{1,0:T(8,128)(2,1)S(1)}, bf16[1056,512]{1,0:T(8,128)(2,1)S(1)}, u32[]{:S(2)}, u32[]{:S(2)}) collective-permute-start(bf16[1056,512]{1,0:T(8,128)(2,1)S(1)} %constant_dynamic-update-slice_fusion.10), channel_id=1, source_target_pairs={{0,1},{1,0},{2,3},{3,2},{4,5},{5,4},{6,7},{7,6},{8,9},{9,8},{10,11... | collective-permute-start | bytes 3244040 | tf_op jit(solution)/shard_map/ppermute | solution.py:29
  184.1 28.6 %collective-permute-start.13 = (bf16[1056,512]{1,0:T(8,128)(2,1)}, bf16[1056,512]{1,0:T(8,128)(2,1)S(1)}, u32[]{:S(2)}, u32[]{:S(2)}) collective-permute-start(bf16[1056,512]{1,0:T(8,128)(2,1)} %collective-permute-done.11), channel_id=1, source_target_pairs={{0,1},{1,0},{2,3},{3,2},{4,5},{5,4},{6,7},{7,6},{8,9},{9,8},{10,11... | collective-permute-start | bytes 3244040 | tf_op jit(solution)/shard_map/ppermute | solution.py:29
  237.0 14.0 %collective-permute-start.27 = (bf16[512,512]{1,0:T(8,128)(2,1)S(1)}, bf16[512,512]{1,0:T(8,128)(2,1)S(1)}, u32[]{:S(2)}, u32[]{:S(2)}) collective-permute-start(bf16[512,512]{1,0:T(8,128)(2,1)S(1)} %get-tuple-element.12), channel_id=1, source_target_pairs={{0,2},{1,3},{2,0},{3,1},{4,6},{5,7},{6,4},{7,5},{8,10},{9,11},{10,... | collective-permute-start | bytes 1572872 | tf_op jit(solution)/shard_map/ppermute | solution.py:196
  237.6 14.8 %collective-permute-start.28 = (bf16[512,512]{1,0:T(8,128)(2,1)S(1)}, bf16[512,512]{1,0:T(8,128)(2,1)S(1)}, u32[]{:S(2)}, u32[]{:S(2)}) collective-permute-start(bf16[512,512]{1,0:T(8,128)(2,1)S(1)} %get-tuple-element.14), channel_id=1, source_target_pairs={{0,4},{1,5},{2,6},{3,7},{4,0},{5,1},{6,2},{7,3},{8,12},{9,13},{10,... | collective-permute-start | bytes 1572872 | tf_op jit(solution)/shard_map/ppermute | solution.py:196
  237.6 25.9 %collective-permute-start.29 = (bf16[512,512]{1,0:T(8,128)(2,1)S(1)}, bf16[512,512]{1,0:T(8,128)(2,1)S(1)}, u32[]{:S(2)}, u32[]{:S(2)}) collective-permute-start(bf16[512,512]{1,0:T(8,128)(2,1)S(1)} %get-tuple-element.13), channel_id=1, source_target_pairs={{0,6},{1,7},{2,4},{3,5},{4,2},{5,3},{6,0},{7,1},{8,14},{9,15},{10,... | collective-permute-start | bytes 1572872 | tf_op jit(solution)/shard_map/ppermute | solution.py:196
  (16 other events, 128.1 us)

commit v2 on v0

v2 whole, which is shorter than its diff:
```python
import functools

import jax
import jax.numpy as jnp
from jax import lax
from jax.experimental import pallas as pl
from jax.experimental.pallas import tpu as pltpu
from jax.sharding import PartitionSpec as P


H = 8
KVH = 2
HD = 128
WINDOW = 128
CONV = 3
HALO = 16


SWAP = [(0, 1), (1, 0)]


def send(cells, axis, pairs):
    return lax.ppermute(cells, axis, pairs)


def xor_pairs(count, mask):
    return [(i, i ^ mask) for i in range(count)]


def attend(queries, keys, values, sink):
    tokens = queries.shape[0]
    heads_here = sink.shape[0]
    levels = lax.axis_size("sp")
    group = H // KVH
    scale = HD ** (-0.5)
    kv_head = (lax.axis_index("tp") * heads_here) // group
    own_keys = lax.dynamic_slice_in_dim(keys, kv_head * HD, HD, 1)
    own_values = lax.dynamic_slice_in_dim(values, kv_head * HD, HD, 1)
    both = jnp.stack([own_keys, own_values])
    up = [(i, i + 1) for i in range(levels - 1)]
    down = [(i + 1, i) for i in range(levels - 1)]
    before = send(both[:, tokens - WINDOW :], "sp", up)
    after = send(both[:, :WINDOW], "sp", down)
    extended = jnp.concatenate([before, both, after], axis=1)
    span = tokens + 2 * WINDOW
    q_heads = queries.reshape(tokens, heads_here, HD)
    scores = (
        jnp.einsum("qhd,kd->hqk", q_heads, extended[0], preferred_element_type=jnp.float32) * scale
    )
    offset = lax.axis_index("sp") * tokens
    q_pos = offset + jnp.arange(tokens, dtype=jnp.int32)[:, None]
    k_pos = offset - WINDOW + jnp.arange(span, dtype=jnp.int32)[None, :]
    valid = (jnp.abs(q_pos - k_pos) <= WINDOW) & (k_pos >= 0) & (k_pos < tokens * levels)
    scores = jnp.where(valid[None], scores, jnp.float32(-1e30))
    sink_col = sink[:, None]
    top = jnp.maximum(jnp.max(scores, axis=-1), sink_col)
    expo = jnp.exp(scores - top[..., None])
    total = jnp.sum(expo, axis=-1) + jnp.exp(sink_col - top)
    weights = (expo / total[..., None]).astype(jnp.bfloat16)
    mixed = jnp.einsum("hqk,kd->qhd", weights, extended[1], preferred_element_type=jnp.float32)
    return mixed.astype(jnp.bfloat16).reshape(tokens, heads_here * HD)


def gather_tp(block):
    count = lax.axis_size("tp")
    slots = {0: block}
    mask = count // 2
    while mask:
        for j in sorted(slots):
            slots[j ^ mask] = send(slots[j], "tp", xor_pairs(count, mask))
        mask //= 2
    return slots


def side_by_side(slots):
    count, tp = lax.axis_size("tp"), lax.axis_index("tp")
    rows, cols = slots[0].shape
    full = jnp.zeros((rows, count * cols), slots[0].dtype)
    for j, block in slots.items():
        full = lax.dynamic_update_slice(full, block, (0, (tp ^ j) * cols))
    return full


def normalize(queries, keys, values, sink, resid, out_proj, norm_gain):
    _, width = resid.shape
    count, tp = lax.axis_size("tp"), lax.axis_index("tp")
    cols = width // count
    mixed = attend(queries, keys, values, sink)
    all_heads = side_by_side(gather_tp(mixed))
    resid_own = lax.dynamic_slice_in_dim(resid, tp * cols, cols, 1)
    gain_own = lax.dynamic_slice_in_dim(norm_gain, tp * cols, cols, 0)
    summed = resid_own.astype(jnp.float32) + jnp.dot(
        all_heads, out_proj, preferred_element_type=jnp.float32
    )
    sums = jnp.stack([jnp.sum(summed, axis=-1), jnp.sum(summed * summed, axis=-1)])
    totals = sums
    for j in range(1, count):
        totals = totals + send(sums, "tp", xor_pairs(count, j))
    mean = (totals[0] / width)[:, None]
    msq = (totals[1] / width)[:, None]
    return ((summed - mean) * lax.rsqrt(msq - mean * mean + 1e-05) * gain_own).astype(
        jnp.bfloat16
    )


def shards(
    queries, keys, values, sink, resid, out_proj, norm_gain, w_gate, w_up, conv_w, conv_b, w_down
):
    fits = lax.axis_size("sp") == lax.axis_size("tp") == 4 and lax.axis_size("grp") == 2
    run = layer_of_four if fits else layer
    return run(
        queries, keys, values, sink, resid, out_proj, norm_gain,
        w_gate, w_up, conv_w, conv_b, w_down,
    )


def spread(full, piece_of, put):
    levels, level, part = lax.axis_size("sp"), lax.axis_index("sp"), lax.axis_index("grp")
    side = level // (levels // 2)
    for share in range(2):
        full = put(full, piece_of(side, share), level, share)
    for mask in range(1, levels):
        cells = piece_of((level ^ mask) // (levels // 2), part)
        got = send(cells, "sp", xor_pairs(levels, mask))
        other = send(got, "grp", SWAP)
        full = put(full, got, level ^ mask, part)
        full = put(full, other, level ^ mask, 1 - part)
    return full


def layer(
    queries, keys, values, sink, resid, out_proj, norm_gain, w_gate, w_up, conv_w, conv_b, w_down
):
    tokens = queries.shape[0]
    width = resid.shape[1]
    levels = lax.axis_size("sp")
    count = lax.axis_size("tp")
    level = lax.axis_index("sp")
    tp = lax.axis_index("tp")
    side = level // (levels // 2)
    cols = width // count
    rows_lv = width // levels
    half = w_gate.shape[1] // 2
    quarter = half // 2

    def gu_piece(of_side, share):
        rows = rows_lv // 2
        return jnp.concatenate(
            [
                lax.dynamic_slice(w, (share * rows, of_side * half), (rows, half))
                for w in (w_gate, w_up)
            ],
            axis=1,
        )

    def put_gu(full, piece, origin, share):
        return lax.dynamic_update_slice(full, piece[None, None], (origin, share, 0, 0))

    def d_piece(of_side, share):
        return lax.dynamic_slice(w_down, (of_side * half + share * quarter, 0), (quarter, rows_lv))

    per = levels // count

    def put_d(full, piece, origin, share):
        slot = (origin // per) ^ tp
        place = (slot >> 1) + (slot & 1) * (count // 2)
        return lax.dynamic_update_slice(
            full, piece[None, None], (place, share, 0, (origin % per) * rows_lv)
        )

    gu_full = jnp.zeros((levels, 2, rows_lv // 2, 2 * half), w_gate.dtype)
    gu_full = spread(gu_full, gu_piece, put_gu)
    gu_full = gu_full.reshape(width, 2 * half)
    d_full = jnp.zeros((count, 2, quarter, cols), w_down.dtype)
    d_full = spread(d_full, d_piece, put_d)
    d_full = d_full.reshape(count, half, cols)

    normed = normalize(queries, keys, values, sink, resid, out_proj, norm_gain)

    mate = levels // 2
    up = [(i, i + 1) for i in range(levels - 1)]
    down = [(i + 1, i) for i in range(levels - 1)]
    tail, head = normed[tokens - HALO :], normed[:HALO]
    other = send(normed, "sp", xor_pairs(levels, mate))
    own_before = send(tail, "sp", up)
    own_after = send(head, "sp", down)
    other_before = send(tail, "sp", [(a, b ^ mate) for a, b in up])
    other_after = send(head, "sp", [(a, b ^ mate) for a, b in down])
    pack = jnp.concatenate([other_before, other, other_after, own_before, own_after])
    normed_own = side_by_side(gather_tp(normed))
    normed_pack = side_by_side(gather_tp(pack))

    taps = lax.dynamic_slice_in_dim(conv_w, side * half, half, 1)
    bias = lax.dynamic_slice_in_dim(conv_b, side * half, half, 0)
    own_gu = jnp.dot(normed_own, gu_full, preferred_element_type=jnp.float32).astype(jnp.bfloat16)
    pack_gu = jnp.dot(normed_pack, gu_full, preferred_element_type=jnp.float32).astype(
        jnp.bfloat16
    )
    around = tokens + 2 * HALO

    def activate(gate, up_part):
        first = HALO - CONV // 2
        conv = bias
        for tap in range(CONV):
            conv = conv + gate[first + tap : first + tap + tokens].astype(jnp.float32) * taps[tap]
        return (jax.nn.silu(conv) * up_part.astype(jnp.float32)).astype(jnp.bfloat16)

    own_gate = jnp.concatenate(
        [pack_gu[around : around + HALO, :half], own_gu[:, :half], pack_gu[around + HALO :, :half]]
    )
    act_own = activate(own_gate, own_gu[:, half:])
    act_other = activate(pack_gu[:around, :half], pack_gu[HALO : HALO + tokens, half:])

    def partial(act, place):
        return jnp.dot(act, d_full[place], preferred_element_type=jnp.float32)

    def over_tp(act):
        pairs_here = count // 2
        away = [partial(act, pairs_here + i).astype(jnp.bfloat16) for i in range(pairs_here)]
        came = send(jnp.stack(away), "tp", xor_pairs(count, 1))
        here = [partial(act, i) + came[i].astype(jnp.float32) for i in range(pairs_here)]
        total = here[0]
        for i in range(1, pairs_here):
            block = send(here[i].astype(jnp.bfloat16), "tp", xor_pairs(count, 2 * i))
            total = total + block.astype(jnp.float32)
        return total

    sum_other = over_tp(act_other).astype(jnp.bfloat16)
    back = send(sum_other, "sp", xor_pairs(levels, mate))
    sum_own = over_tp(act_own)
    return (normed.astype(jnp.float32) + sum_own + back.astype(jnp.float32)).astype(jnp.bfloat16)


def gate_up_kernel(
    x0, x1, x2, x3, o0, o1, o2, o3, e0, e1, e2, e3, w_gate, w_up, z1, y1, z2, y2, z3, y3, taps, bias,
    out, xs, es, ws, gate, sems,
):
    tokens, cols = x0.shape
    half = taps.shape[1]
    rows = z1.shape[0]
    level, tp, part = lax.axis_index("sp"), lax.axis_index("tp"), lax.axis_index("grp")
    odd = level & 1
    copies = []

    def copy(source, target):
        item = pltpu.make_async_copy(source, target, sems.at[len(copies)])
        item.start()
        copies.append(item)

    copy(w_gate.at[:, pl.ds(pl.multiple_of(odd * half, half), half)], ws.at[0:cols, 0:half])
    copy(w_up.at[:, pl.ds(pl.multiple_of(odd * half, half), half)], ws.at[0:cols, half : 2 * half])
    own_rows = pl.ds(pl.multiple_of(odd * tokens, tokens), tokens)
    other_rows = pl.ds(pl.multiple_of((1 - odd) * tokens, tokens), tokens)
    columns = ((x0, o0, e0), (x1, o1, e1), (x2, o2, e2), (x3, o3, e3))
    for j, (mine, other, edge) in enumerate(columns):
        lanes = pl.ds(pl.multiple_of((tp ^ j ^ level) * cols, cols), cols)
        copy(mine, xs.at[own_rows, lanes])
        copy(other, xs.at[other_rows, lanes])
        copy(edge, es.at[:, lanes])
    for mask, (z, y) in enumerate(((z1, y1), (z2, y2), (z3, y3)), 1):
        base = mask * cols
        copy(z, ws.at[pl.ds(pl.multiple_of(base + part * rows, rows), rows), :])
        copy(y, ws.at[pl.ds(pl.multiple_of(base + (1 - part) * rows, rows), rows), :])
    for item in copies:
        item.wait()

    step = 256
    around = jnp.dot(es[...], ws[:, :half], preferred_element_type=jnp.float32)
    around = around.astype(jnp.bfloat16).astype(jnp.float32)
    even = odd == 0
    gate[7:8, :] = jnp.where(even, around[HALO - 1 : HALO], around[2 * HALO - 1 : 2 * HALO])
    gate[8 + 2 * tokens : 9 + 2 * tokens, :] = jnp.where(even, around[HALO : HALO + 1], around[0:1])

    def gates(i, carry):
        cells = xs[pl.ds(pl.multiple_of(i * step, step), step), :]
        acc = jnp.dot(cells, ws[:, :half], preferred_element_type=jnp.float32)
        gate[pl.ds(pl.multiple_of(8 + i * step, 8), step), :] = acc.astype(jnp.bfloat16).astype(
            jnp.float32
        )
        return carry

    lax.fori_loop(0, 2 * tokens // step, gates, 0)
    for start in range(0, 2 * tokens, step):
        cells = xs[start : start + step, :]
        acc = jnp.dot(cells, ws[:, half:], preferred_element_type=jnp.float32)
        up_part = acc.astype(jnp.bfloat16).astype(jnp.float32)
        conv = bias[...]
        for tap in range(CONV):
            conv = conv + gate[7 + tap + start : 7 + tap + start + step, :] * taps[tap : tap + 1, :]
        silu = conv / (1.0 + jnp.exp(-conv))
        out[start : start + step, :] = (silu * up_part).astype(jnp.bfloat16)


def gate_up(own, other, edges, w_gate, w_up, pieces, taps, bias):
    tokens, cols = own[0].shape
    half = taps.shape[1]
    width = 4 * cols
    near, far = pl.BlockSpec(memory_space=pl.ANY), pl.BlockSpec(memory_space=pltpu.VMEM)
    return pl.pallas_call(
        gate_up_kernel,
        out_shape=jax.ShapeDtypeStruct((2 * tokens, half), jnp.bfloat16),
        in_specs=[near] * 20 + [far] * 2,
        out_specs=far,
        scratch_shapes=[
            pltpu.VMEM((2 * tokens, width), jnp.bfloat16),
            pltpu.VMEM((2 * HALO, width), jnp.bfloat16),
            pltpu.VMEM((width, 2 * half), jnp.bfloat16),
            pltpu.VMEM((2 * tokens + HALO, half), jnp.float32),
            pltpu.SemaphoreType.DMA((20,)),
        ],
        compiler_params=pltpu.CompilerParams(vmem_limit_bytes=40 * 2**20),
        name="gate_up",
    )(*own, *other, *edges, w_gate, w_up, *pieces, taps, bias)


def down_kernel(parity, act, w_down, z1, y1, z2, y2, z3, y3, out, ds, sems):
    tokens, _ = out.shape[2:]
    half = act.shape[1]
    quarter = half // 2
    level, tp, part = lax.axis_index("sp"), lax.axis_index("tp"), lax.axis_index("grp")
    odd = level & 1
    lower = pl.ds(pl.multiple_of(part * quarter, quarter), quarter)
    upper = pl.ds(pl.multiple_of((1 - part) * quarter, quarter), quarter)
    copies = []
    for mask in range(4):
        slot = level ^ mask ^ tp
        if mask == 0:
            own = w_down.at[pl.ds(pl.multiple_of(odd * half, half), half), :]
            parts = [(own, ds.at[slot])]
        else:
            z, y = ((z1, y1), (z2, y2), (z3, y3))[mask - 1]
            parts = [(z, ds.at[slot, lower, :]), (y, ds.at[slot, upper, :])]
        for source, target in parts:
            item = pltpu.make_async_copy(source, target, sems.at[len(copies)])
            item.start()
            copies.append(item)
    for item in copies:
        item.wait()
    for which in range(2):
        block = odd if which else 1 - odd
        cells = act[pl.ds(pl.multiple_of(block * tokens, tokens), tokens), :]
        for i in range(2):
            out[which, i] = jnp.dot(
                cells, ds[2 * i + parity], preferred_element_type=jnp.float32
            ).astype(out.dtype)


def down(act, w_down, pieces, parity, dtype):
    tokens, half = act.shape[0] // 2, act.shape[1]
    cols = w_down.shape[1]
    near, far = pl.BlockSpec(memory_space=pl.ANY), pl.BlockSpec(memory_space=pltpu.VMEM)
    return pl.pallas_call(
        functools.partial(down_kernel, parity),
        out_shape=jax.ShapeDtypeStruct((2, 2, tokens, cols), dtype),
        in_specs=[far] + [near] * 7,
        out_specs=far,
        scratch_shapes=[pltpu.VMEM((4, half, cols), jnp.bfloat16), pltpu.SemaphoreType.DMA((7,))],
        compiler_params=pltpu.CompilerParams(vmem_limit_bytes=24 * 2**20),
    )(act, w_down, *pieces)


def travel(piece_of):
    odd, part = lax.axis_index("sp") & 1, lax.axis_index("grp")
    pieces = []
    for mask in range(1, 4):
        z = send(piece_of(odd ^ (mask & 1), part), "sp", xor_pairs(4, mask))
        pieces += [z, send(z, "grp", SWAP)]
    return pieces


def layer_of_four(
    queries, keys, values, sink, resid, out_proj, norm_gain, w_gate, w_up, conv_w, conv_b, w_down
):
    tokens = queries.shape[0]
    odd = lax.axis_index("sp") & 1
    half = w_gate.shape[1] // 2
    quarter = half // 2

    def gu_piece(of_side, share):
        rows = w_gate.shape[0] // 2
        return jnp.concatenate(
            [
                lax.dynamic_slice(w, (share * rows, of_side * half), (rows, half))
                for w in (w_gate, w_up)
            ],
            axis=1,
        )

    def d_piece(of_side, share):
        return lax.dynamic_slice(
            w_down, (of_side * half + share * quarter, 0), (quarter, w_down.shape[1])
        )

    gu = travel(gu_piece)
    dn = travel(d_piece)
    normed = normalize(queries, keys, values, sink, resid, out_proj, norm_gain)
    mate = send(normed, "sp", xor_pairs(4, 1))
    outer = jnp.where(odd == 1, normed[tokens - HALO :], normed[:HALO])
    near = send(outer, "sp", [(1, 2), (2, 1)])
    far = send(outer, "sp", [(1, 3), (2, 0)])
    own = gather_tp(normed)
    other = gather_tp(mate)
    edges = gather_tp(jnp.concatenate([near, far]))

    taps = lax.dynamic_slice_in_dim(conv_w, odd * half, half, 1)
    bias = lax.dynamic_slice_in_dim(conv_b, odd * half, half, 0)
    act = gate_up(
        *([slots[j] for j in range(4)] for slots in (own, other, edges)),
        w_gate, w_up, gu, taps, bias[None],
    )

    away = down(act, w_down, dn, 1, jnp.bfloat16)
    came = [send(away[i], "tp", xor_pairs(4, 1)) for i in range(2)]
    here = down(act, w_down, dn, 0, jnp.float32)

    middle = tokens // 2

    def partial(which, slot, rows):
        return here[which, slot, rows] + came[which][slot, rows].astype(jnp.float32)

    def cross(cells, axis, mask):
        return send(cells.astype(jnp.bfloat16), axis, xor_pairs(4, mask)).astype(jnp.float32)

    top, low = slice(0, middle), slice(middle, tokens)
    x_other = cross(partial(0, 1, top), "tp", 2)
    z_low = cross(jnp.stack([partial(0, 0, low), partial(0, 1, low)]), "sp", 1)
    x_top = cross(partial(1, 1, top), "tp", 2)
    back = cross(partial(0, 0, top) + x_other, "sp", 1)
    x_low = cross(partial(1, 1, low) + z_low[1], "tp", 2)
    ffn = jnp.concatenate([partial(1, 0, top) + x_top + back, partial(1, 0, low) + z_low[0] + x_low])
    return (normed.astype(jnp.float32) + ffn).astype(jnp.bfloat16)


def solution(mesh):
    step = jax.shard_map(
        shards,
        mesh=mesh,
        in_specs=(
            P(("grp", "sp"), "tp"),
            P(("grp", "sp"), None),
            P(("grp", "sp"), None),
            P("tp"),
            P(("grp", "sp"), None),
            P(None, "tp"),
            P(),
            P("sp", "tp"),
            P("sp", "tp"),
            P(None, "tp"),
            P("tp"),
            P("tp", "sp"),
        ),
        out_specs=P(("grp", "sp"), "tp"),
        check_vma=False,
    )
    if not (mesh.shape["sp"] == mesh.shape["tp"] == 4 and mesh.shape["grp"] == 2):
        return step
    return step
```

time: 476 us -> 251 us (0.53)
  waiting for transfers between devices: 418 us -> 170 us
  starting transfers between devices: 9.21 us -> 41.8 us
  matrix products: 29.4 us -> 4.84 us
  Pallas kernels: 0 us -> 18.2 us
  between operations: 13.7 us -> 0.43 us
  local copies, waits for them, and re-layouts: 1.13 us -> 7.48 us
    all_gather x5 -> x0, waiting for transfers between devices: 382 us -> none  [the longest x1 115 us: shards(): lax.all_gather(w_down, 'sp', axis=1, tiled=True)]
    ppermute x4 -> x39, waiting for transfers between devices: 4.03 us -> 170 us  [send(): return lax.ppermute(cells, axis, pairs)]
    ppermute x4 -> x39, starting transfers between devices: 9.01 us -> 41.8 us  [send(): return lax.ppermute(cells, axis, pairs)]
    reduce_scatter x1 -> x0, waiting for transfers between devices: 29.5 us -> none  [shards(): lax.psum_scatter(terms.astype(jnp.bfloat16), 'tp', scatter_dimension=1, t...]
    dot_general x5 -> x3, matrix products: 29.4 us -> 4.84 us  [the longest x1 2.93 us: normalize(): jnp.dot(all_heads, out_proj, preferred_element_type=jnp.float32)]
    pallas_call x0 -> x3, Pallas kernels: none -> 18.2 us  [the longest x1 12.1 us: gate_up(): pl.pallas_call(gate_up_kernel, out_shape=jax.ShapeDtypeStruct((2 * tokens...]
  transfers between devices with their start and end apart: 10 -> 39, of which waited for: 7 -> 20; matrix products, arithmetic and copies ran while one was open for 3% -> 4% of each run, Pallas kernels for 0% -> 6%
where the time goes in v2:
time: 251 us; the launch traced here: 250 us
  waiting for transfers between devices  170 us (68%)
  starting transfers between devices  41.8 us (17%)
  Pallas kernels  18.2 us (7%)
  local copies, waits for them, and re-layouts  7.48 us (3%)
  other arithmetic  7.19 us (3%)
  matrix products  4.84 us (2%)
    ppermute x39, waiting for transfers between devices, send(): return lax.ppermute(cells, axis, pairs)  170 us
    ppermute x39, starting transfers between devices, send(): return lax.ppermute(cells, axis, pairs)  41.8 us
    pallas_call x1, Pallas kernels, gate_up(): pl.pallas_call(gate_up_kernel, out_shape=jax.ShapeDtypeStruct((2 * tokens...  12.1 us
    pallas_call x2, Pallas kernels, down(): pl.pallas_call(functools.partial(down_kernel, parity), out_shape=jax.Shap...  6.1 us
  transfers between devices with their start and end apart: 39, of which 20 were waited for; matrix products, arithmetic and copies ran while one was open for 4% of the time, Pallas kernels for 6%

profile of v2, /device:TPU:0, one launch (start us, length us, event | category | flops | bytes accessed | tf_op | source)
XLA Modules:
  0.0 250.2 jit_solution(3857373771805339391)
XLA Ops:
  1.1 5.0 %collective-permute-start = (bf16[2,128,128]{2,1,0:T(8,128)(2,1)S(1)}, bf16[2,128,128]{2,1,0:T(8,128)(2,1)S(1)}, u32[]{:S(2)}, u32[]{:S(2)}) collective-permute-start(bf16[2,128,128]{2,1,0:T(8,128)(2,1)S(1)} %get-tuple-element.21), channel_id=1, source_target_pairs={{0,4},{4,8},{8,12},{1,5},{5,9},{9,13},{2,6},{6,10},{10,14},{3,7},{... | collective-permute-start | bytes 196616 | tf_op jit(solution)/shard_map/ppermute | solution.py:23
  9.7 2.5 %collective-permute-done.1 = bf16[2,128,128]{2,1,0:T(8,128)(2,1)S(1)} collective-permute-done((bf16[2,128,128]{2,1,0:T(8,128)(2,1)S(1)}, bf16[2,128,128]{2,1,0:T(8,128)(2,1)S(1)}, u32[]{:S(2)}, u32[]{:S(2)}) %collective-permute-start.1) | collective-permute-done | bytes 65568 | tf_op jit(solution)/shard_map/ppermute | solution.py:23
  19.2 2.5 collective-permute-start.24
  24.3 2.9 %fusion.34 = (f32[512]{0:T(512)S(1)}, f32[512]{0:T(512)S(1)}, f32[512,512]{1,0:T(8,128)}) fusion(bf16[512,1024]{0,1:T(8,128)(2,1)S(1)} %constant_dynamic-update-slice_fusion.2, bf16[1024,512]{1,0:T(8,128)(2,1)S(1)} %copy-done, bf16[512,2048]{1,0:T(8,128)(2,1)} %param.16, s32[]{:T(128)S(6)} %select_n.64), kind=kOutput, calls=%fused_computation.89 | convolution fusion | flops 538180608 | bytes 3674116 | tf_op jit(solution)/shard_map/dot_general | solution.py:92
  31.5 2.5 collective-permute-start.30
  35.9 26.9 %collective-permute-done.26.z1 = bf16[384,512]{1,0:T(8,128)(2,1)S(1)} collective-permute-done((bf16[384,512]{1,0:T(8,128)(2,1)}, bf16[384,512]{1,0:T(8,128)(2,1)S(1)}, u32[]{:S(2)}, u32[]{:S(2)}) %collective-permute-start.26) | collective-permute-done | bytes 393248 | tf_op jit(solution)/shard_map/ppermute | solution.py:23
  62.7 5.6 %collective-permute-start.28 = (bf16[384,512]{1,0:T(8,128)(2,1)}, bf16[384,512]{1,0:T(8,128)(2,1)S(1)}, u32[]{:S(2)}, u32[]{:S(2)}) collective-permute-start(bf16[384,512]{1,0:T(8,128)(2,1)} %get-tuple-element.15), channel_id=1, source_target_pairs={{0,8},{4,12},{8,0},{12,4},{1,9},{5,13},{9,1},{13,5},{2,10},{6,14},... | collective-permute-start | bytes 1179656 | tf_op jit(solution)/shard_map/ppermute | solution.py:23
  68.4 5.7 %collective-permute-done.30.z3 = bf16[384,512]{1,0:T(8,128)(2,1)S(1)} collective-permute-done((bf16[384,512]{1,0:T(8,128)(2,1)}, bf16[384,512]{1,0:T(8,128)(2,1)S(1)}, u32[]{:S(2)}, u32[]{:S(2)}) %collective-permute-start.30) | collective-permute-done | bytes 393248 | tf_op jit(solution)/shard_map/ppermute | solution.py:23
  76.3 50.1 %collective-permute-done.16 = bf16[16,512]{1,0:T(8,128)(2,1)S(1)} collective-permute-done((bf16[16,512]{1,0:T(8,128)(2,1)S(1)}, bf16[16,512]{1,0:T(8,128)(2,1)S(1)}, u32[]{:S(2)}, u32[]{:S(2)}) %collective-permute-start.16) | collective-permute-done | bytes 16416 | tf_op jit(solution)/shard_map/ppermute | solution.py:23
  127.0 3.4 %collective-permute-done.18.e2 = bf16[32,512]{1,0:T(8,128)(2,1)S(1)} collective-permute-done((bf16[32,512]{1,0:T(8,128)(2,1)S(1)}, bf16[32,512]{1,0:T(8,128)(2,1)S(1)}, u32[]{:S(2)}, u32[]{:S(2)}) %collective-permute-start.18) | collective-permute-done | bytes 32800 | tf_op jit(solution)/shard_map/ppermute | solution.py:23
  138.5 8.3 %collective-permute-done.9.x2 = bf16[512,512]{1,0:T(8,128)(2,1)S(1)} collective-permute-done((bf16[512,512]{1,0:T(8,128)(2,1)S(1)}, bf16[512,512]{1,0:T(8,128)(2,1)S(1)}, u32[]{:S(2)}, u32[]{:S(2)}) %collective-permute-start.9) | collective-permute-done | bytes 524320 | tf_op jit(solution)/shard_map/ppermute | solution.py:23
  147.3 6.5 %collective-permute-done.21.y1 = bf16[256,1536]{1,0:T(8,128)(2,1)S(1)} collective-permute-done((bf16[256,1536]{1,0:T(8,128)(2,1)S(1)}, bf16[256,1536]{1,0:T(8,128)(2,1)S(1)}, u32[]{:S(2)}, u32[]{:S(2)}) %collective-permute-start.21) | collective-permute-done | bytes 786464 | tf_op jit(solution)/shard_map/ppermute | solution.py:23
  153.8 6.1 %collective-permute-done.13.o2 = bf16[512,512]{1,0:T(8,128)(2,1)S(1)} collective-permute-done((bf16[512,512]{1,0:T(8,128)(2,1)S(1)}, bf16[512,512]{1,0:T(8,128)(2,1)S(1)}, u32[]{:S(2)}, u32[]{:S(2)}) %collective-permute-start.13) | collective-permute-done | bytes 524320 | tf_op jit(solution)/shard_map/ppermute | solution.py:23
  159.9 10.8 %collective-permute-done.25.y3 = bf16[256,1536]{1,0:T(8,128)(2,1)S(1)} collective-permute-done((bf16[256,1536]{1,0:T(8,128)(2,1)}, bf16[256,1536]{1,0:T(8,128)(2,1)S(1)}, u32[]{:S(2)}, u32[]{:S(2)}) %collective-permute-start.25) | collective-permute-done | bytes 786464 | tf_op jit(solution)/shard_map/ppermute | solution.py:23
  172.2 15.3 %collective-permute-done.23.y2 = bf16[256,1536]{1,0:T(8,128)(2,1)S(1)} collective-permute-done((bf16[256,1536]{1,0:T(8,128)(2,1)S(1)}, bf16[256,1536]{1,0:T(8,128)(2,1)S(1)}, u32[]{:S(2)}, u32[]{:S(2)}) %collective-permute-start.23) | collective-permute-done | bytes 786464 | tf_op jit(solution)/shard_map/ppermute | solution.py:23
  192.5 12.1 %gate_up.1.act = bf16[1024,768]{1,0:T(8,128)(2,1)S(1)} custom-call(bf16[512,512]{1,0:T(8,128)(2,1)S(1)} %multiply_convert_fusion.x0, bf16[512,512]{1,0:T(8,128)(2,1)S(1)} %collective-permute-done.8.x1, bf16[512,512]{1,0:T(8,128)(2,1)S(1)} %collective-permute-done.9.x2, bf16[512,512]{1,0:T(8,128)(2,1)S(1)} %collective-permute-done.10.x3, ...), custom_call_target="tpu_custom_call" | custom-call | tf_op jit(solution)/shard_map/gate_up/pallas_call | solution.py:299
  204.6 7.7 %collective-permute-done.29.y2 = bf16[384,512]{1,0:T(8,128)(2,1)S(1)} collective-permute-done((bf16[384,512]{1,0:T(8,128)(2,1)S(1)}, bf16[384,512]{1,0:T(8,128)(2,1)S(1)}, u32[]{:S(2)}, u32[]{:S(2)}) %collective-permute-start.29) | collective-permute-done | bytes 393248 | tf_op jit(solution)/shard_map/ppermute | solution.py:23
  212.3 3.0 %shard_map.119 = bf16[2,2,512,512]{3,2,1,0:T(8,128)(2,1)S(1)} custom-call(bf16[1024,768]{1,0:T(8,128)(2,1)S(1)} %gate_up.1.act, bf16[1536,512]{1,0:T(8,128)(2,1)S(1)} %copy-done.1, bf16[384,512]{1,0:T(8,128)(2,1)S(1)} %collective-permute-done.26.z1, bf16[384,512]{1,0:T(8,128)(2,1)S(1)} %collective-permute-done.27.y1, ...), custom_call_target="tpu_custom_call" | custom-call | tf_op jit(solution)/shard_map/pallas_call | solution.py:352
  216.1 3.0 %shard_map.118 = f32[2,2,512,512]{3,2,1,0:T(8,128)S(1)} custom-call(bf16[1024,768]{1,0:T(8,128)(2,1)S(1)} %gate_up.1.act, bf16[1536,512]{1,0:T(8,128)(2,1)S(1)} %copy-done.1, bf16[384,512]{1,0:T(8,128)(2,1)S(1)} %collective-permute-done.26.z1, bf16[384,512]{1,0:T(8,128)(2,1)S(1)} %collective-permute-done.27.y1, ...), custom_call_target="tpu_custom_call" | custom-call | tf_op jit(solution)/shard_map/pallas_call | solution.py:352
  224.2 4.9 %collective-permute-done.35 = bf16[256,512]{1,0:T(8,128)(2,1)S(1)} collective-permute-done((bf16[256,512]{1,0:T(8,128)(2,1)S(1)}, bf16[256,512]{1,0:T(8,128)(2,1)S(1)}, u32[]{:S(2)}, u32[]{:S(2)}) %collective-permute-start.35) | collective-permute-done | bytes 262176 | tf_op jit(solution)/shard_map/ppermute | solution.py:23
  229.2 2.0 collective-permute-start.36
  231.3 5.3 %collective-permute-done.37 = bf16[2,256,512]{2,1,0:T(8,128)(2,1)S(1)} collective-permute-done((bf16[2,256,512]{2,1,0:T(8,128)(2,1)S(1)}, bf16[2,256,512]{2,1,0:T(8,128)(2,1)S(1)}, u32[]{:S(2)}, u32[]{:S(2)}) %collective-permute-start.37) | collective-permute-done | bytes 524320 | tf_op jit(solution)/shard_map/ppermute | solution.py:23
  236.7 4.6 %collective-permute-done.36 = bf16[256,512]{1,0:T(8,128)(2,1)S(1)} collective-permute-done((bf16[256,512]{1,0:T(8,128)(2,1)S(1)}, bf16[256,512]{1,0:T(8,128)(2,1)S(1)}, u32[]{:S(2)}, u32[]{:S(2)}) %collective-permute-start.36) | collective-permute-done | bytes 262176 | tf_op jit(solution)/shard_map/ppermute | solution.py:23
  242.1 6.9 %collective-permute-done.38 = bf16[256,512]{1,0:T(8,128)(2,1)S(1)} collective-permute-done((bf16[256,512]{1,0:T(8,128)(2,1)S(1)}, bf16[256,512]{1,0:T(8,128)(2,1)S(1)}, u32[]{:S(2)}, u32[]{:S(2)}) %collective-permute-start.38) | collective-permute-done | bytes 262176 | tf_op jit(solution)/shard_map/ppermute | solution.py:23
  (118 shorter events, 46.3 us)
Async XLA Ops:
  17.6 115.7 %collective-permute-start.20 = (bf16[256,1536]{1,0:T(8,128)(2,1)}, bf16[256,1536]{1,0:T(8,128)(2,1)S(1)}, u32[]{:S(2)}, u32[]{:S(2)}) collective-permute-start(bf16[256,1536]{1,0:T(8,128)(2,1)} %pad_maximum_fusion), channel_id=1, source_target_pairs={{0,4},{4,0},{8,12},{12,8},{1,5},{5,1},{9,13},{13,9},{2,6},{6,2},{1... | collective-permute-start | bytes 2359304 | tf_op jit(solution)/shard_map/ppermute | solution.py:23
  19.2 114.2 %collective-permute-start.24 = (bf16[256,1536]{1,0:T(8,128)(2,1)}, bf16[256,1536]{1,0:T(8,128)(2,1)}, u32[]{:S(2)}, u32[]{:S(2)}) collective-permute-start(bf16[256,1536]{1,0:T(8,128)(2,1)} %pad_maximum_fusion), channel_id=1, source_target_pairs={{0,12},{4,8},{8,4},{12,0},{1,13},{5,9},{9,5},{13,1},{2,14},{6,10},... | collective-permute-start | bytes 2359304 | tf_op jit(solution)/shard_map/ppermute | solution.py:23
  30.9 31.9 %collective-permute-start.26 = (bf16[384,512]{1,0:T(8,128)(2,1)}, bf16[384,512]{1,0:T(8,128)(2,1)S(1)}, u32[]{:S(2)}, u32[]{:S(2)}) collective-permute-start(bf16[384,512]{1,0:T(8,128)(2,1)} %get-tuple-element.16), channel_id=1, source_target_pairs={{0,4},{4,0},{8,12},{12,8},{1,5},{5,1},{9,13},{13,9},{2,6},{6,2},{1... | collective-permute-start | bytes 1179656 | tf_op jit(solution)/shard_map/ppermute | solution.py:23
  31.5 42.6 %collective-permute-start.30 = (bf16[384,512]{1,0:T(8,128)(2,1)}, bf16[384,512]{1,0:T(8,128)(2,1)S(1)}, u32[]{:S(2)}, u32[]{:S(2)}) collective-permute-start(bf16[384,512]{1,0:T(8,128)(2,1)} %get-tuple-element.16), channel_id=1, source_target_pairs={{0,12},{4,8},{8,4},{12,0},{1,13},{5,9},{9,5},{13,1},{2,14},{6,10},... | collective-permute-start | bytes 1179656 | tf_op jit(solution)/shard_map/ppermute | solution.py:23
  34.0 100.9 %collective-permute-start.22 = (bf16[256,1536]{1,0:T(8,128)(2,1)}, bf16[256,1536]{1,0:T(8,128)(2,1)S(1)}, u32[]{:S(2)}, u32[]{:S(2)}) collective-permute-start(bf16[256,1536]{1,0:T(8,128)(2,1)} %pad_maximum_fusion.1), channel_id=1, source_target_pairs={{0,8},{4,12},{8,0},{12,4},{1,9},{5,13},{9,1},{13,5},{2,10},{6,14},... | collective-permute-start | bytes 2359304 | tf_op jit(solution)/shard_map/ppermute | solution.py:23
  62.7 63.7 %collective-permute-start.28 = (bf16[384,512]{1,0:T(8,128)(2,1)}, bf16[384,512]{1,0:T(8,128)(2,1)S(1)}, u32[]{:S(2)}, u32[]{:S(2)}) collective-permute-start(bf16[384,512]{1,0:T(8,128)(2,1)} %get-tuple-element.15), channel_id=1, source_target_pairs={{0,8},{4,12},{8,0},{12,4},{1,9},{5,13},{9,1},{13,5},{2,10},{6,14},... | collective-permute-start | bytes 1179656 | tf_op jit(solution)/shard_map/ppermute | solution.py:23
  74.8 51.6 %collective-permute-start.16 = (bf16[16,512]{1,0:T(8,128)(2,1)S(1)}, bf16[16,512]{1,0:T(8,128)(2,1)S(1)}, u32[]{:S(2)}, u32[]{:S(2)}) collective-permute-start(bf16[16,512]{1,0:T(8,128)(2,1)S(1)} %slice_select_fusion), channel_id=1, source_target_pairs={{4,12},{8,0},{5,13},{9,1},{6,14},{10,2},{7,15},{11,3},{20,28},{24,... | collective-permute-start | bytes 49160 | tf_op jit(solution)/shard_map/ppermute | solution.py:23
  126.4 10.6 %collective-permute-start.11 = (bf16[512,512]{1,0:T(8,128)(2,1)S(1)}, bf16[512,512]{1,0:T(8,128)(2,1)S(1)}, u32[]{:S(2)}, u32[]{:S(2)}) collective-permute-start(bf16[512,512]{1,0:T(8,128)(2,1)S(1)} %multiply_convert_fusion.x0), channel_id=1, source_target_pairs={{0,4},{4,0},{8,12},{12,8},{1,5},{5,1},{9,13},{13,9},{2,6},{6,2},{1... | collective-permute-start | bytes 1572872 | tf_op jit(solution)/shard_map/ppermute | solution.py:23
  132.8 14.0 %collective-permute-start.9 = (bf16[512,512]{1,0:T(8,128)(2,1)S(1)}, bf16[512,512]{1,0:T(8,128)(2,1)S(1)}, u32[]{:S(2)}, u32[]{:S(2)}) collective-permute-start(bf16[512,512]{1,0:T(8,128)(2,1)S(1)} %multiply_convert_fusion.x0), channel_id=1, source_target_pairs={{0,2},{1,3},{2,0},{3,1},{4,6},{5,7},{6,4},{7,5},{8,10},{9,11},{10,... | collective-permute-start | bytes 1572872 | tf_op jit(solution)/shard_map/ppermute | solution.py:23
  133.3 14.0 %collective-permute-start.8 = (bf16[512,512]{1,0:T(8,128)(2,1)S(1)}, bf16[512,512]{1,0:T(8,128)(2,1)S(1)}, u32[]{:S(2)}, u32[]{:S(2)}) collective-permute-start(bf16[512,512]{1,0:T(8,128)(2,1)S(1)} %multiply_convert_fusion.x0), channel_id=1, source_target_pairs={{0,1},{1,0},{2,3},{3,2},{4,5},{5,4},{6,7},{7,6},{8,9},{9,8},{10,11... | collective-permute-start | bytes 1572872 | tf_op jit(solution)/shard_map/ppermute | solution.py:23
  133.4 20.5 %collective-permute-start.21 = (bf16[256,1536]{1,0:T(8,128)(2,1)S(1)}, bf16[256,1536]{1,0:T(8,128)(2,1)S(1)}, u32[]{:S(2)}, u32[]{:S(2)}) collective-permute-start(bf16[256,1536]{1,0:T(8,128)(2,1)S(1)} %collective-permute-done.20.z1), channel_id=1, source_target_pairs={{0,16},{16,0},{1,17},{17,1},{2,18},{18,2},{3,19},{19,3},{4,20},{20... | collective-permute-start | bytes 2359304 | tf_op jit(solution)/shard_map/ppermute | solution.py:23
  134.9 35.7 %collective-permute-start.25 = (bf16[256,1536]{1,0:T(8,128)(2,1)}, bf16[256,1536]{1,0:T(8,128)(2,1)S(1)}, u32[]{:S(2)}, u32[]{:S(2)}) collective-permute-start(bf16[256,1536]{1,0:T(8,128)(2,1)} %collective-permute-done.24.z3), channel_id=1, source_target_pairs={{0,16},{16,0},{1,17},{17,1},{2,18},{18,2},{3,19},{19,3},{4,20},{20... | collective-permute-start | bytes 2359304 | tf_op jit(solution)/shard_map/ppermute | solution.py:23
  137.0 50.5 %collective-permute-start.23 = (bf16[256,1536]{1,0:T(8,128)(2,1)S(1)}, bf16[256,1536]{1,0:T(8,128)(2,1)S(1)}, u32[]{:S(2)}, u32[]{:S(2)}) collective-permute-start(bf16[256,1536]{1,0:T(8,128)(2,1)S(1)} %collective-permute-done.22.z2), channel_id=1, source_target_pairs={{0,16},{16,0},{1,17},{17,1},{2,18},{18,2},{3,19},{19,3},{4,20},{20... | collective-permute-start | bytes 2359304 | tf_op jit(solution)/shard_map/ppermute | solution.py:23
  146.8 13.1 %collective-permute-start.13 = (bf16[512,512]{1,0:T(8,128)(2,1)S(1)}, bf16[512,512]{1,0:T(8,128)(2,1)S(1)}, u32[]{:S(2)}, u32[]{:S(2)}) collective-permute-start(bf16[512,512]{1,0:T(8,128)(2,1)S(1)} %collective-permute-done.11.o0), channel_id=1, source_target_pairs={{0,2},{1,3},{2,0},{3,1},{4,6},{5,7},{6,4},{7,5},{8,10},{9,11},{10,... | collective-permute-start | bytes 1572872 | tf_op jit(solution)/shard_map/ppermute | solution.py:23
  147.3 41.7 %collective-permute-start.10 = (bf16[512,512]{1,0:T(8,128)(2,1)S(1)}, bf16[512,512]{1,0:T(8,128)(2,1)S(1)}, u32[]{:S(2)}, u32[]{:S(2)}) collective-permute-start(bf16[512,512]{1,0:T(8,128)(2,1)S(1)} %collective-permute-done.9.x2), channel_id=1, source_target_pairs={{0,1},{1,0},{2,3},{3,2},{4,5},{5,4},{6,7},{7,6},{8,9},{9,8},{10,11... | collective-permute-start | bytes 1572872 | tf_op jit(solution)/shard_map/ppermute | solution.py:23
  153.8 35.8 %collective-permute-start.12 = (bf16[512,512]{1,0:T(8,128)(2,1)S(1)}, bf16[512,512]{1,0:T(8,128)(2,1)S(1)}, u32[]{:S(2)}, u32[]{:S(2)}) collective-permute-start(bf16[512,512]{1,0:T(8,128)(2,1)S(1)} %collective-permute-done.11.o0), channel_id=1, source_target_pairs={{0,1},{1,0},{2,3},{3,2},{4,5},{5,4},{6,7},{7,6},{8,9},{9,8},{10,11... | collective-permute-start | bytes 1572872 | tf_op jit(solution)/shard_map/ppermute | solution.py:23
  159.9 29.7 %collective-permute-start.14 = (bf16[512,512]{1,0:T(8,128)(2,1)S(1)}, bf16[512,512]{1,0:T(8,128)(2,1)S(1)}, u32[]{:S(2)}, u32[]{:S(2)}) collective-permute-start(bf16[512,512]{1,0:T(8,128)(2,1)S(1)} %collective-permute-done.13.o2), channel_id=1, source_target_pairs={{0,1},{1,0},{2,3},{3,2},{4,5},{5,4},{6,7},{7,6},{8,9},{9,8},{10,11... | collective-permute-start | bytes 1572872 | tf_op jit(solution)/shard_map/ppermute | solution.py:23
  170.7 33.9 %collective-permute-start.27 = (bf16[384,512]{1,0:T(8,128)(2,1)S(1)}, bf16[384,512]{1,0:T(8,128)(2,1)S(1)}, u32[]{:S(2)}, u32[]{:S(2)}) collective-permute-start(bf16[384,512]{1,0:T(8,128)(2,1)S(1)} %collective-permute-done.26.z1), channel_id=1, source_target_pairs={{0,16},{16,0},{1,17},{17,1},{2,18},{18,2},{3,19},{19,3},{4,20},{20... | collective-permute-start | bytes 1179656 | tf_op jit(solution)/shard_map/ppermute | solution.py:23
  187.5 17.1 %collective-permute-start.31 = (bf16[384,512]{1,0:T(8,128)(2,1)S(1)}, bf16[384,512]{1,0:T(8,128)(2,1)S(1)}, u32[]{:S(2)}, u32[]{:S(2)}) collective-permute-start(bf16[384,512]{1,0:T(8,128)(2,1)S(1)} %collective-permute-done.30.z3), channel_id=1, source_target_pairs={{0,16},{16,0},{1,17},{17,1},{2,18},{18,2},{3,19},{19,3},{4,20},{20... | collective-permute-start | bytes 1179656 | tf_op jit(solution)/shard_map/ppermute | solution.py:23
  189.1 23.2 %collective-permute-start.29 = (bf16[384,512]{1,0:T(8,128)(2,1)S(1)}, bf16[384,512]{1,0:T(8,128)(2,1)S(1)}, u32[]{:S(2)}, u32[]{:S(2)}) collective-permute-start(bf16[384,512]{1,0:T(8,128)(2,1)S(1)} %collective-permute-done.28.z2), channel_id=1, source_target_pairs={{0,16},{16,0},{1,17},{17,1},{2,18},{18,2},{3,19},{19,3},{4,20},{20... | collective-permute-start | bytes 1179656 | tf_op jit(solution)/shard_map/ppermute | solution.py:23
  219.9 9.2 %collective-permute-start.35 = (bf16[256,512]{1,0:T(8,128)(2,1)S(1)}, bf16[256,512]{1,0:T(8,128)(2,1)S(1)}, u32[]{:S(2)}, u32[]{:S(2)}) collective-permute-start(bf16[256,512]{1,0:T(8,128)(2,1)S(1)} %get-tuple-element.12), channel_id=1, source_target_pairs={{0,2},{1,3},{2,0},{3,1},{4,6},{5,7},{6,4},{7,5},{8,10},{9,11},{10,... | collective-permute-start | bytes 786440 | tf_op jit(solution)/shard_map/ppermute | solution.py:23
  221.7 14.9 %collective-permute-start.37 = (bf16[2,256,512]{2,1,0:T(8,128)(2,1)S(1)}, bf16[2,256,512]{2,1,0:T(8,128)(2,1)S(1)}, u32[]{:S(2)}, u32[]{:S(2)}) collective-permute-start(bf16[2,256,512]{2,1,0:T(8,128)(2,1)S(1)} %pad_maximum_fusion.2), channel_id=1, source_target_pairs={{0,4},{4,0},{8,12},{12,8},{1,5},{5,1},{9,13},{13,9},{2,6},{6,2},{1... | collective-permute-start | bytes 1572872 | tf_op jit(solution)/shard_map/ppermute | solution.py:23
  223.7 13.0 %collective-permute-start.33 = (bf16[256,512]{1,0:T(8,128)(2,1)S(1)}, bf16[256,512]{1,0:T(8,128)(2,1)S(1)}, u32[]{:S(2)}, u32[]{:S(2)}) collective-permute-start(bf16[256,512]{1,0:T(8,128)(2,1)S(1)} %get-tuple-element.11), channel_id=1, source_target_pairs={{0,2},{1,3},{2,0},{3,1},{4,6},{5,7},{6,4},{7,5},{8,10},{9,11},{10,... | collective-permute-start | bytes 786440 | tf_op jit(solution)/shard_map/ppermute | solution.py:23
  229.2 12.0 %collective-permute-start.36 = (bf16[256,512]{1,0:T(8,128)(2,1)S(1)}, bf16[256,512]{1,0:T(8,128)(2,1)S(1)}, u32[]{:S(2)}, u32[]{:S(2)}) collective-permute-start(bf16[256,512]{1,0:T(8,128)(2,1)S(1)} %fusion.21), channel_id=1, source_target_pairs={{0,4},{4,0},{8,12},{12,8},{1,5},{5,1},{9,13},{13,9},{2,6},{6,2},{1... | collective-permute-start | bytes 786440 | tf_op jit(solution)/shard_map/ppermute | solution.py:23
  (24 other events, 445.9 us)

commit v3 on v2

--- a/solution.py
+++ b/solution.py
@@ -1,5 +1,3 @@
-import functools
-
 import jax
 import jax.numpy as jnp
 from jax import lax
@@ -232,11 +230,11 @@
 
 
 def gate_up_kernel(
-    x0, x1, x2, x3, o0, o1, o2, o3, e0, e1, e2, e3, w_gate, w_up, z1, y1, z2, y2, z3, y3, taps, bias,
-    out, xs, es, ws, gate, sems,
+    x0, x1, x2, x3, o0, o1, o2, o3, e0, e1, e2, e3, w_gate, w_up, z1, y1, z2, y2,
+    acc, around, last, xs, es, ws, sems,
 ):
     tokens, cols = x0.shape
-    half = taps.shape[1]
+    half = acc.shape[1] // 2
     rows = z1.shape[0]
     level, tp, part = lax.axis_index("sp"), lax.axis_index("tp"), lax.axis_index("grp")
     odd = level & 1
@@ -247,8 +245,6 @@
         item.start()
         copies.append(item)
 
-    copy(w_gate.at[:, pl.ds(pl.multiple_of(odd * half, half), half)], ws.at[0:cols, 0:half])
-    copy(w_up.at[:, pl.ds(pl.multiple_of(odd * half, half), half)], ws.at[0:cols, half : 2 * half])
     own_rows = pl.ds(pl.multiple_of(odd * tokens, tokens), tokens)
     other_rows = pl.ds(pl.multiple_of((1 - odd) * tokens, tokens), tokens)
     columns = ((x0, o0, e0), (x1, o1, e1), (x2, o2, e2), (x3, o3, e3))
@@ -257,64 +253,128 @@
         copy(mine, xs.at[own_rows, lanes])
         copy(other, xs.at[other_rows, lanes])
         copy(edge, es.at[:, lanes])
-    for mask, (z, y) in enumerate(((z1, y1), (z2, y2), (z3, y3)), 1):
+    for i, w in enumerate((w_gate, w_up)):
+        copy(
+            w.at[:, pl.ds(pl.multiple_of(odd * half, half), half)],
+            ws.at[0:cols, i * half : (i + 1) * half],
+        )
+    for mask, (z, y) in enumerate(((z1, y1), (z2, y2)), 1):
         base = mask * cols
         copy(z, ws.at[pl.ds(pl.multiple_of(base + part * rows, rows), rows), :])
         copy(y, ws.at[pl.ds(pl.multiple_of(base + (1 - part) * rows, rows), rows), :])
     for item in copies:
         item.wait()
-
+    known = 3 * cols
+    around[...] = jnp.dot(es[:, :known], ws[:, :half], preferred_element_type=jnp.float32)
+    last[0 : 2 * tokens, :] = xs[:, known:]
+    last[2 * tokens : 2 * tokens + 2 * HALO, :] = es[:, known:]
     step = 256
-    around = jnp.dot(es[...], ws[:, :half], preferred_element_type=jnp.float32)
-    around = around.astype(jnp.bfloat16).astype(jnp.float32)
-    even = odd == 0
-    gate[7:8, :] = jnp.where(even, around[HALO - 1 : HALO], around[2 * HALO - 1 : 2 * HALO])
-    gate[8 + 2 * tokens : 9 + 2 * tokens, :] = jnp.where(even, around[HALO : HALO + 1], around[0:1])
+
+    def some_rows(i, carry):
+        here = pl.ds(pl.multiple_of(i * step, step), step)
+        acc[here, :] = jnp.dot(xs[here, :known], ws[...], preferred_element_type=jnp.float32)
+        return carry
+
+    lax.fori_loop(0, 2 * tokens // step, some_rows, 0)
+
+
+def gate_up(own, other, edges, w_gate, w_up, pieces):
+    tokens, cols = own[0].shape
+    both = w_gate.shape[1]
+    near, far = pl.BlockSpec(memory_space=pl.ANY), pl.BlockSpec(memory_space=pltpu.VMEM)
+    return pl.pallas_call(
+        gate_up_kernel,
+        out_shape=(
+            jax.ShapeDtypeStruct((2 * tokens, both), jnp.float32),
+            jax.ShapeDtypeStruct((2 * HALO, both // 2), jnp.float32),
+            jax.ShapeDtypeStruct((2 * tokens + 2 * HALO, cols), jnp.bfloat16),
+        ),
+        in_specs=[near] * 18,
+        out_specs=(far, far, far),
+        scratch_shapes=[
+            pltpu.VMEM((2 * tokens, 4 * cols), jnp.bfloat16),
+            pltpu.VMEM((2 * HALO, 4 * cols), jnp.bfloat16),
+            pltpu.VMEM((3 * cols, both), jnp.bfloat16),
+            pltpu.SemaphoreType.DMA((18,)),
+        ],
+        compiler_params=pltpu.CompilerParams(vmem_limit_bytes=32 * 2**20),
+        name="gate_up",
+    )(*own, *other, *edges, w_gate, w_up, *pieces)
+
+
+def activate_kernel(acc, around, last, z3, y3, taps, bias, out, ws, gate, sems):
+    tokens2, both = acc.shape
+    half = both // 2
+    rows = z3.shape[0]
+    level, part = lax.axis_index("sp"), lax.axis_index("grp")
+    copies = [
+        pltpu.make_async_copy(
+            source, ws.at[pl.ds(pl.multiple_of(share * rows, rows), rows), :], sems.at[i]
+        )
+        for i, (source, share) in enumerate(((z3, part), (y3, 1 - part)))
+    ]
+    for item in copies:
+        item.start()
+    for item in copies:
+        item.wait()
+    step = 256
+    ends = around[...] + jnp.dot(
+        last[tokens2:, :], ws[:, :half], preferred_element_type=jnp.float32
+    )
+    ends = ends.astype(jnp.bfloat16).astype(jnp.float32)
+    even = (level & 1) == 0
+    gate[7:8, :] = jnp.where(even, ends[HALO - 1 : HALO], ends[2 * HALO - 1 : 2 * HALO])
+    gate[8 + tokens2 : 9 + tokens2, :] = jnp.where(even, ends[HALO : HALO + 1], ends[0:1])
 
     def gates(i, carry):
-        cells = xs[pl.ds(pl.multiple_of(i * step, step), step), :]
-        acc = jnp.dot(cells, ws[:, :half], preferred_element_type=jnp.float32)
-        gate[pl.ds(pl.multiple_of(8 + i * step, 8), step), :] = acc.astype(jnp.bfloat16).astype(
+        here = pl.ds(pl.multiple_of(i * step, step), step)
+        total = acc[here, :half] + jnp.dot(
+            last[here, :], ws[:, :half], preferred_element_type=jnp.float32
+        )
+        gate[pl.ds(pl.multiple_of(8 + i * step, 8), step), :] = total.astype(jnp.bfloat16).astype(
             jnp.float32
         )
         return carry
 
-    lax.fori_loop(0, 2 * tokens // step, gates, 0)
-    for start in range(0, 2 * tokens, step):
-        cells = xs[start : start + step, :]
-        acc = jnp.dot(cells, ws[:, half:], preferred_element_type=jnp.float32)
-        up_part = acc.astype(jnp.bfloat16).astype(jnp.float32)
+    lax.fori_loop(0, tokens2 // step, gates, 0)
+    for start in range(0, tokens2, step):
+        here = slice(start, start + step)
+        total = acc[here, half:] + jnp.dot(
+            last[here, :], ws[:, half:], preferred_element_type=jnp.float32
+        )
+        up_part = total.astype(jnp.bfloat16).astype(jnp.float32)
         conv = bias[...]
         for tap in range(CONV):
             conv = conv + gate[7 + tap + start : 7 + tap + start + step, :] * taps[tap : tap + 1, :]
         silu = conv / (1.0 + jnp.exp(-conv))
-        out[start : start + step, :] = (silu * up_part).astype(jnp.bfloat16)
-
-
-def gate_up(own, other, edges, w_gate, w_up, pieces, taps, bias):
-    tokens, cols = own[0].shape
+        out[here, :] = (silu * up_part).astype(jnp.bfloat16)
+
+
+def activate_last(sums, pieces, taps, bias):
+    acc, around, last = sums
+    near, far = pl.BlockSpec(memory_space=pl.ANY), pl.BlockSpec(memory_space=pltpu.VMEM)
     half = taps.shape[1]
-    width = 4 * cols
-    near, far = pl.BlockSpec(memory_space=pl.ANY), pl.BlockSpec(memory_space=pltpu.VMEM)
     return pl.pallas_call(
-        gate_up_kernel,
-        out_shape=jax.ShapeDtypeStruct((2 * tokens, half), jnp.bfloat16),
-        in_specs=[near] * 20 + [far] * 2,
+        activate_kernel,
+        out_shape=jax.ShapeDtypeStruct((acc.shape[0], half), jnp.bfloat16),
+        in_specs=[far] * 3 + [near] * 2 + [far] * 2,
         out_specs=far,
         scratch_shapes=[
-            pltpu.VMEM((2 * tokens, width), jnp.bfloat16),
-            pltpu.VMEM((2 * HALO, width), jnp.bfloat16),
-            pltpu.VMEM((width, 2 * half), jnp.bfloat16),
-            pltpu.VMEM((2 * tokens + HALO, half), jnp.float32),
-            pltpu.SemaphoreType.DMA((20,)),
+            pltpu.VMEM((last.shape[1], 2 * half), jnp.bfloat16),
+            pltpu.VMEM((acc.shape[0] + HALO, half), jnp.float32),
+            pltpu.SemaphoreType.DMA((2,)),
         ],
-        compiler_params=pltpu.CompilerParams(vmem_limit_bytes=40 * 2**20),
-        name="gate_up",
-    )(*own, *other, *edges, w_gate, w_up, *pieces, taps, bias)
-
-
-def down_kernel(parity, act, w_down, z1, y1, z2, y2, z3, y3, out, ds, sems):
-    tokens, _ = out.shape[2:]
+        compiler_params=pltpu.CompilerParams(vmem_limit_bytes=32 * 2**20),
+        name="activate",
+    )(acc, around, last, *pieces, taps, bias)
+
+
+def place_of(slot):
+    return (slot >> 1) + 2 * (slot & 1)
+
+
+def down_kernel(act, w_down, z1, y1, z2, y2, away_other, away_own, here, ds, sems):
+    tokens, _ = here.shape[2:]
     half = act.shape[1]
     quarter = half // 2
     level, tp, part = lax.axis_index("sp"), lax.axis_index("tp"), lax.axis_index("grp")
@@ -322,41 +382,110 @@
     lower = pl.ds(pl.multiple_of(part * quarter, quarter), quarter)
     upper = pl.ds(pl.multiple_of((1 - part) * quarter, quarter), quarter)
     copies = []
-    for mask in range(4):
-        slot = level ^ mask ^ tp
-        if mask == 0:
-            own = w_down.at[pl.ds(pl.multiple_of(odd * half, half), half), :]
-            parts = [(own, ds.at[slot])]
-        else:
-            z, y = ((z1, y1), (z2, y2), (z3, y3))[mask - 1]
-            parts = [(z, ds.at[slot, lower, :]), (y, ds.at[slot, upper, :])]
-        for source, target in parts:
-            item = pltpu.make_async_copy(source, target, sems.at[len(copies)])
-            item.start()
-            copies.append(item)
+
+    def copy(source, target):
+        item = pltpu.make_async_copy(source, target, sems.at[len(copies)])
+        item.start()
+        copies.append(item)
+
+    copy(
+        w_down.at[pl.ds(pl.multiple_of(odd * half, half), half), :],
+        ds.at[place_of(level ^ tp)],
+    )
+    for mask, (z, y) in enumerate(((z1, y1), (z2, y2)), 1):
+        place = place_of(level ^ mask ^ tp)
+        copy(z, ds.at[place, lower, :])
+        copy(y, ds.at[place, upper, :])
     for item in copies:
+        item.wait()
+    for which, away in ((0, away_other), (1, away_own)):
+        block = odd if which else 1 - odd
+        cells = act[pl.ds(pl.multiple_of(block * tokens, tokens), tokens), :]
+        for i in range(2):
+            away[i] = jnp.dot(cells, ds[2 + i], preferred_element_type=jnp.float32).astype(
+                away.dtype
+            )
+            here[which, i] = jnp.dot(cells, ds[i], preferred_element_type=jnp.float32).astype(
+                here.dtype
+            )
+
+
+def down_last_kernel(
+    act, z3, y3, away_other_in, away_own_in, here_in, away_other, away_own, here, ds, sums, sems
+):
+    del away_other_in, away_own_in, here_in
+    tokens = sums.shape[1]
+    half = act.shape[1]
+    quarter = half // 2
+    level, tp, part = lax.axis_index("sp"), lax.axis_index("tp"), lax.axis_index("grp")
+    odd = level & 1
+    slot = level ^ 3 ^ tp
+    loads = [
+        pltpu.make_async_copy(
+            source, ds.at[pl.ds(pl.multiple_of(share * quarter, quarter), quarter), :], sems.at[i]
+        )
+        for i, (source, share) in enumerate(((z3, part), (y3, 1 - part)))
+    ]
+    for item in loads:
+        item.start()
+    for item in loads:
         item.wait()
     for which in range(2):
         block = odd if which else 1 - odd
         cells = act[pl.ds(pl.multiple_of(block * tokens, tokens), tokens), :]
-        for i in range(2):
-            out[which, i] = jnp.dot(
-                cells, ds[2 * i + parity], preferred_element_type=jnp.float32
-            ).astype(out.dtype)
-
-
-def down(act, w_down, pieces, parity, dtype):
+        sums[which] = jnp.dot(cells, ds[...], preferred_element_type=jnp.float32).astype(sums.dtype)
+
+    def store(targets):
+        stores = [
+            pltpu.make_async_copy(sums.at[which], target, sems.at[2 + which])
+            for which, target in enumerate(targets)
+        ]
+        for item in stores:
+            item.start()
+        for item in stores:
+            item.wait()
+
+    @pl.when((slot & 1) == 1)
+    def _():
+        store((away_other.at[slot >> 1], away_own.at[slot >> 1]))
+
+    @pl.when((slot & 1) == 0)
+    def _():
+        store((here.at[0, slot >> 1], here.at[1, slot >> 1]))
+
+
+def down(act, w_down, pieces):
     tokens, half = act.shape[0] // 2, act.shape[1]
     cols = w_down.shape[1]
     near, far = pl.BlockSpec(memory_space=pl.ANY), pl.BlockSpec(memory_space=pltpu.VMEM)
+    shapes = (
+        jax.ShapeDtypeStruct((2, tokens, cols), jnp.bfloat16),
+        jax.ShapeDtypeStruct((2, tokens, cols), jnp.bfloat16),
+        jax.ShapeDtypeStruct((2, 2, tokens, cols), jnp.bfloat16),
+    )
+    known = pl.pallas_call(
+        down_kernel,
+        out_shape=shapes,
+        in_specs=[far] + [near] * 5,
+        out_specs=(far, far, far),
+        scratch_shapes=[pltpu.VMEM((4, half, cols), jnp.bfloat16), pltpu.SemaphoreType.DMA((5,))],
+        compiler_params=pltpu.CompilerParams(vmem_limit_bytes=24 * 2**20),
+        name="down",
+    )(act, w_down, *pieces[:4])
     return pl.pallas_call(
-        functools.partial(down_kernel, parity),
-        out_shape=jax.ShapeDtypeStruct((2, 2, tokens, cols), dtype),
-        in_specs=[far] + [near] * 7,
-        out_specs=far,
-        scratch_shapes=[pltpu.VMEM((4, half, cols), jnp.bfloat16), pltpu.SemaphoreType.DMA((7,))],
-        compiler_params=pltpu.CompilerParams(vmem_limit_bytes=24 * 2**20),
-    )(act, w_down, *pieces)
+        down_last_kernel,
+        out_shape=shapes,
+        in_specs=[far] + [near] * 5,
+        out_specs=(near, near, near),
+        input_output_aliases={3: 0, 4: 1, 5: 2},
+        scratch_shapes=[
+            pltpu.VMEM((half, cols), jnp.bfloat16),
+            pltpu.VMEM((2, tokens, cols), jnp.bfloat16),
+            pltpu.SemaphoreType.DMA((4,)),
+        ],
+        compiler_params=pltpu.CompilerParams(vmem_limit_bytes=16 * 2**20),
+        name="down_last",
+    )(act, *pieces[4:], *known)
 
 
 def travel(piece_of):
@@ -404,19 +533,18 @@
 
     taps = lax.dynamic_slice_in_dim(conv_w, odd * half, half, 1)
     bias = lax.dynamic_slice_in_dim(conv_b, odd * half, half, 0)
-    act = gate_up(
-        *([slots[j] for j in range(4)] for slots in (own, other, edges)),
-        w_gate, w_up, gu, taps, bias[None],
-    )
-
-    away = down(act, w_down, dn, 1, jnp.bfloat16)
-    came = [send(away[i], "tp", xor_pairs(4, 1)) for i in range(2)]
-    here = down(act, w_down, dn, 0, jnp.float32)
+    sums = gate_up(
+        *([slots[j] for j in range(4)] for slots in (own, other, edges)), w_gate, w_up, gu[:4]
+    )
+    act = activate_last(sums, gu[4:], taps, bias[None])
+
+    away_other, away_own, here = down(act, w_down, dn)
+    came = [send(away_other, "tp", xor_pairs(4, 1)), send(away_own, "tp", xor_pairs(4, 1))]
 
     middle = tokens // 2
 
     def partial(which, slot, rows):
-        return here[which, slot, rows] + came[which][slot, rows].astype(jnp.float32)
+        return here[which, slot, rows].astype(jnp.float32) + came[which][slot, rows].astype(jnp.float32)
 
     def cross(cells, axis, mask):
         return send(cells.astype(jnp.bfloat16), axis, xor_pairs(4, mask)).astype(jnp.float32)
@@ -426,7 +554,8 @@
     z_low = cross(jnp.stack([partial(0, 0, low), partial(0, 1, low)]), "sp", 1)
     x_top = cross(partial(1, 1, top), "tp", 2)
     back = cross(partial(0, 0, top) + x_other, "sp", 1)
-    x_low = cross(partial(1, 1, low) + z_low[1], "tp", 2)
+    low_sum = (partial(1, 1, low) + z_low[1]).astype(jnp.bfloat16)
+    x_low = cross(low_sum, "tp", 2)
     ffn = jnp.concatenate([partial(1, 0, top) + x_top + back, partial(1, 0, low) + z_low[0] + x_low])
     return (normed.astype(jnp.float32) + ffn).astype(jnp.bfloat16)
 

time: 251 us -> 237 us (0.944)
  waiting for transfers between devices: 170 us -> 160 us
  starting transfers between devices: 41.8 us -> 39 us
    ppermute x39, waiting for transfers between devices: 170 us -> 160 us  [send(): return lax.ppermute(cells, axis, pairs)]
    ppermute x39, starting transfers between devices: 41.8 us -> 39 us  [send(): return lax.ppermute(cells, axis, pairs)]
    pallas_call x3 -> x4, Pallas kernels: 18.2 us -> 18.9 us  [the longest x1 8.18 us: gate_up(): pl.pallas_call(gate_up_kernel, out_shape=(jax.ShapeDtypeStruct((2 * token...]
  transfers between devices with their start and end apart: 39 -> 39, of which waited for: 20 -> 22; matrix products, arithmetic and copies ran while one was open for 4% -> 5% of each run, Pallas kernels for 6% -> 7%
where the time goes in v3:
time: 237 us
  waiting for transfers between devices  160 us (68%)
  starting transfers between devices  39 us (16%)
  Pallas kernels  18.9 us (8%)
  other arithmetic  7.07 us (3%)
  local copies, waits for them, and re-layouts  6.04 us (3%)
  matrix products  4.83 us (2%)
    ppermute x39, waiting for transfers between devices, send(): return lax.ppermute(cells, axis, pairs)  160 us
    ppermute x39, starting transfers between devices, send(): return lax.ppermute(cells, axis, pairs)  39 us
    pallas_call x1, Pallas kernels, gate_up(): pl.pallas_call(gate_up_kernel, out_shape=(jax.ShapeDtypeStruct((2 * token...  8.18 us
    pallas_call x1, Pallas kernels, activate_last(): pl.pallas_call(activate_kernel, out_shape=jax.ShapeDtypeStruct((acc.shape...  4.97 us
  transfers between devices with their start and end apart: 39, of which 22 were waited for; matrix products, arithmetic and copies ran while one was open for 5% of the time, Pallas kernels for 7%

profile of v3, /device:TPU:0, one launch (start us, length us, event | category | flops | bytes accessed | tf_op | source)
XLA Modules:
  0.0 236.7 jit_solution(9464274084772722198)
XLA Ops:
  1.1 5.0 %collective-permute-start = (bf16[2,128,128]{2,1,0:T(8,128)(2,1)S(1)}, bf16[2,128,128]{2,1,0:T(8,128)(2,1)S(1)}, u32[]{:S(2)}, u32[]{:S(2)}) collective-permute-start(bf16[2,128,128]{2,1,0:T(8,128)(2,1)S(1)} %get-tuple-element.37), channel_id=1, source_target_pairs={{0,4},{4,8},{8,12},{1,5},{5,9},{9,13},{2,6},{6,10},{10,14},{3,7},{... | collective-permute-start | bytes 196616 | tf_op jit(solution)/shard_map/ppermute | solution.py:21
  9.7 2.5 %collective-permute-done.1 = bf16[2,128,128]{2,1,0:T(8,128)(2,1)S(1)} collective-permute-done((bf16[2,128,128]{2,1,0:T(8,128)(2,1)S(1)}, bf16[2,128,128]{2,1,0:T(8,128)(2,1)S(1)}, u32[]{:S(2)}, u32[]{:S(2)}) %collective-permute-start.1) | collective-permute-done | bytes 65568 | tf_op jit(solution)/shard_map/ppermute | solution.py:21
  19.2 2.5 %collective-permute-start.24 = (bf16[256,1536]{1,0:T(8,128)(2,1)}, bf16[256,1536]{1,0:T(8,128)(2,1)S(1)}, u32[]{:S(2)}, u32[]{:S(2)}) collective-permute-start(bf16[256,1536]{1,0:T(8,128)(2,1)} %pad_maximum_fusion), channel_id=1, source_target_pairs={{0,12},{4,8},{8,4},{12,0},{1,13},{5,9},{9,5},{13,1},{2,14},{6,10},... | collective-permute-start | bytes 2359304 | tf_op jit(solution)/shard_map/ppermute | solution.py:21
  24.3 2.9 %fusion.26 = (f32[512]{0:T(512)S(1)}, f32[512]{0:T(512)S(1)}, f32[512,512]{1,0:T(8,128)}) fusion(bf16[512,1024]{0,1:T(8,128)(2,1)S(1)} %constant_dynamic-update-slice_fusion.2, bf16[1024,512]{1,0:T(8,128)(2,1)S(1)} %copy-done, bf16[512,2048]{1,0:T(8,128)(2,1)} %param.16, s32[]{:T(128)S(6)} %select_n.64), kind=kOutput, calls=%fused_computation.79 | convolution fusion | flops 538180608 | bytes 3674116 | tf_op jit(solution)/shard_map/dot_general | solution.py:90
  36.0 43.6 %collective-permute-done.28.z1 = bf16[384,512]{1,0:T(8,128)(2,1)S(1)} collective-permute-done((bf16[384,512]{1,0:T(8,128)(2,1)}, bf16[384,512]{1,0:T(8,128)(2,1)S(1)}, u32[]{:S(2)}, u32[]{:S(2)}) %collective-permute-start.28) | collective-permute-done | bytes 393248 | tf_op jit(solution)/shard_map/ppermute | solution.py:21
  79.6 2.5 %collective-permute-start.26 = (bf16[384,512]{1,0:T(8,128)(2,1)}, bf16[384,512]{1,0:T(8,128)(2,1)S(1)}, u32[]{:S(2)}, u32[]{:S(2)}) collective-permute-start(bf16[384,512]{1,0:T(8,128)(2,1)} %get-tuple-element.32), channel_id=1, source_target_pairs={{0,12},{4,8},{8,4},{12,0},{1,13},{5,9},{9,5},{13,1},{2,14},{6,10},... | collective-permute-start | bytes 1179656 | tf_op jit(solution)/shard_map/ppermute | solution.py:21
  82.1 32.8 %collective-permute-done.30.z2 = bf16[384,512]{1,0:T(8,128)(2,1)S(1)} collective-permute-done((bf16[384,512]{1,0:T(8,128)(2,1)}, bf16[384,512]{1,0:T(8,128)(2,1)S(1)}, u32[]{:S(2)}, u32[]{:S(2)}) %collective-permute-start.30) | collective-permute-done | bytes 393248 | tf_op jit(solution)/shard_map/ppermute | solution.py:21
  117.0 9.4 %collective-permute-done.16 = bf16[16,512]{1,0:T(8,128)(2,1)S(1)} collective-permute-done((bf16[16,512]{1,0:T(8,128)(2,1)S(1)}, bf16[16,512]{1,0:T(8,128)(2,1)S(1)}, u32[]{:S(2)}, u32[]{:S(2)}) %collective-permute-start.16) | collective-permute-done | bytes 16416 | tf_op jit(solution)/shard_map/ppermute | solution.py:21
  128.5 3.4 %collective-permute-done.18.e2 = bf16[32,512]{1,0:T(8,128)(2,1)S(1)} collective-permute-done((bf16[32,512]{1,0:T(8,128)(2,1)S(1)}, bf16[32,512]{1,0:T(8,128)(2,1)S(1)}, u32[]{:S(2)}, u32[]{:S(2)}) %collective-permute-start.18) | collective-permute-done | bytes 32800 | tf_op jit(solution)/shard_map/ppermute | solution.py:21
  137.8 11.2 %collective-permute-done.9.x2 = bf16[512,512]{1,0:T(8,128)(2,1)S(1)} collective-permute-done((bf16[512,512]{1,0:T(8,128)(2,1)S(1)}, bf16[512,512]{1,0:T(8,128)(2,1)S(1)}, u32[]{:S(2)}, u32[]{:S(2)}) %collective-permute-start.9) | collective-permute-done | bytes 524320 | tf_op jit(solution)/shard_map/ppermute | solution.py:21
  150.1 9.4 %collective-permute-done.13.o2 = bf16[512,512]{1,0:T(8,128)(2,1)S(1)} collective-permute-done((bf16[512,512]{1,0:T(8,128)(2,1)S(1)}, bf16[512,512]{1,0:T(8,128)(2,1)S(1)}, u32[]{:S(2)}, u32[]{:S(2)}) %collective-permute-start.13) | collective-permute-done | bytes 524320 | tf_op jit(solution)/shard_map/ppermute | solution.py:21
  159.5 4.4 %collective-permute-done.23.y2 = bf16[256,1536]{1,0:T(8,128)(2,1)S(1)} collective-permute-done((bf16[256,1536]{1,0:T(8,128)(2,1)S(1)}, bf16[256,1536]{1,0:T(8,128)(2,1)S(1)}, u32[]{:S(2)}, u32[]{:S(2)}) %collective-permute-start.23) | collective-permute-done | bytes 786464 | tf_op jit(solution)/shard_map/ppermute | solution.py:21
  168.9 8.2 %gate_up.1 = (f32[1024,1536]{1,0:T(8,128)S(1)}, f32[32,768]{1,0:T(8,128)S(1)}, bf16[1056,512]{1,0:T(8,128)(2,1)S(1)}) custom-call(bf16[512,512]{1,0:T(8,128)(2,1)S(1)} %multiply_convert_fusion.x0, bf16[512,512]{1,0:T(8,128)(2,1)S(1)} %collective-permute-done.8.x1, bf16[512,512]{1,0:T(8,128)(2,1)S(1)} %collective-permute-done.9.x2, ...), custom_call_target="tpu_custom_call" | custom-call | tf_op jit(solution)/shard_map/gate_up/pallas_call | solution.py:285
  177.1 3.6 %collective-permute-done.25.y3 = bf16[256,1536]{1,0:T(8,128)(2,1)S(1)} collective-permute-done((bf16[256,1536]{1,0:T(8,128)(2,1)S(1)}, bf16[256,1536]{1,0:T(8,128)(2,1)S(1)}, u32[]{:S(2)}, u32[]{:S(2)}) %collective-permute-start.25) | collective-permute-done | bytes 786464 | tf_op jit(solution)/shard_map/ppermute | solution.py:21
  180.7 5.0 %activate.1.act = bf16[1024,768]{1,0:T(8,128)(2,1)S(1)} custom-call(f32[1024,1536]{1,0:T(8,128)S(1)} %get-tuple-element.14.acc, f32[32,768]{1,0:T(8,128)S(1)} %get-tuple-element.15.around, bf16[1056,512]{1,0:T(8,128)(2,1)S(1)} %get-tuple-element.16.last, bf16[256,1536]{1,0:T(8,128)(2,1)S(1)} %collective-permute-done.24.z3, ...), custom_call_target="tpu_custom_call" | custom-call | tf_op jit(solution)/shard_map/activate/pallas_call | solution.py:357
  185.7 3.4 %collective-permute-done.29.y1 = bf16[384,512]{1,0:T(8,128)(2,1)S(1)} collective-permute-done((bf16[384,512]{1,0:T(8,128)(2,1)S(1)}, bf16[384,512]{1,0:T(8,128)(2,1)S(1)}, u32[]{:S(2)}, u32[]{:S(2)}) %collective-permute-start.29) | collective-permute-done | bytes 393248 | tf_op jit(solution)/shard_map/ppermute | solution.py:21
  189.1 8.4 %collective-permute-done.31.y2 = bf16[384,512]{1,0:T(8,128)(2,1)S(1)} collective-permute-done((bf16[384,512]{1,0:T(8,128)(2,1)S(1)}, bf16[384,512]{1,0:T(8,128)(2,1)S(1)}, u32[]{:S(2)}, u32[]{:S(2)}) %collective-permute-start.31) | collective-permute-done | bytes 393248 | tf_op jit(solution)/shard_map/ppermute | solution.py:21
  197.6 4.3 %down.1 = (bf16[2,512,512]{2,1,0:T(8,128)(2,1)S(1)}, bf16[2,512,512]{2,1,0:T(8,128)(2,1)S(1)}, bf16[2,2,512,512]{3,2,1,0:T(8,128)(2,1)S(1)}) custom-call(bf16[1024,768]{1,0:T(8,128)(2,1)S(1)} %activate.1.act, bf16[1536,512]{1,0:T(8,128)(2,1)S(1)} %copy-done.1, bf16[384,512]{1,0:T(8,128)(2,1)S(1)} %collective-permute-done.28.z1, ...), custom_call_target="tpu_custom_call" | custom-call | tf_op jit(solution)/shard_map/down/pallas_call | solution.py:466
  204.0 2.1 collective-permute-done.32
  212.0 5.0 %collective-permute-done.35 = bf16[256,512]{1,0:T(8,128)(2,1)S(1)} collective-permute-done((bf16[256,512]{1,0:T(8,128)(2,1)S(1)}, bf16[256,512]{1,0:T(8,128)(2,1)S(1)}, u32[]{:S(2)}, u32[]{:S(2)}) %collective-permute-start.35) | collective-permute-done | bytes 262176 | tf_op jit(solution)/shard_map/ppermute | solution.py:21
  217.1 1.9 collective-permute-start.36
  219.0 4.4 %collective-permute-done.37 = bf16[2,256,512]{2,1,0:T(8,128)(2,1)S(1)} collective-permute-done((bf16[2,256,512]{2,1,0:T(8,128)(2,1)S(1)}, bf16[2,256,512]{2,1,0:T(8,128)(2,1)S(1)}, u32[]{:S(2)}, u32[]{:S(2)}) %collective-permute-start.37) | collective-permute-done | bytes 524320 | tf_op jit(solution)/shard_map/ppermute | solution.py:21
  223.6 4.4 %collective-permute-done.36 = bf16[256,512]{1,0:T(8,128)(2,1)S(1)} collective-permute-done((bf16[256,512]{1,0:T(8,128)(2,1)S(1)}, bf16[256,512]{1,0:T(8,128)(2,1)S(1)}, u32[]{:S(2)}, u32[]{:S(2)}) %collective-permute-start.36) | collective-permute-done | bytes 262176 | tf_op jit(solution)/shard_map/ppermute | solution.py:21
  229.8 5.6 %collective-permute-done.38 = bf16[256,512]{1,0:T(8,128)(2,1)S(1)} collective-permute-done((bf16[256,512]{1,0:T(8,128)(2,1)S(1)}, bf16[256,512]{1,0:T(8,128)(2,1)S(1)}, u32[]{:S(2)}, u32[]{:S(2)}) %collective-permute-start.38) | collective-permute-done | bytes 262176 | tf_op jit(solution)/shard_map/ppermute | solution.py:21
  (118 shorter events, 50.4 us)
Async XLA Ops:
  1.1 8.6 %collective-permute-start = (bf16[2,128,128]{2,1,0:T(8,128)(2,1)S(1)}, bf16[2,128,128]{2,1,0:T(8,128)(2,1)S(1)}, u32[]{:S(2)}, u32[]{:S(2)}) collective-permute-start(bf16[2,128,128]{2,1,0:T(8,128)(2,1)S(1)} %get-tuple-element.37), channel_id=1, source_target_pairs={{0,4},{4,8},{8,12},{1,5},{5,9},{9,13},{2,6},{6,10},{10,14},{3,7},{... | collective-permute-start | bytes 196616 | tf_op jit(solution)/shard_map/ppermute | solution.py:21
  17.6 108.8 %collective-permute-start.20 = (bf16[256,1536]{1,0:T(8,128)(2,1)}, bf16[256,1536]{1,0:T(8,128)(2,1)}, u32[]{:S(2)}, u32[]{:S(2)}) collective-permute-start(bf16[256,1536]{1,0:T(8,128)(2,1)} %pad_maximum_fusion), channel_id=1, source_target_pairs={{0,4},{4,0},{8,12},{12,8},{1,5},{5,1},{9,13},{13,9},{2,6},{6,2},{1... | collective-permute-start | bytes 2359304 | tf_op jit(solution)/shard_map/ppermute | solution.py:21
  19.2 115.6 %collective-permute-start.24 = (bf16[256,1536]{1,0:T(8,128)(2,1)}, bf16[256,1536]{1,0:T(8,128)(2,1)S(1)}, u32[]{:S(2)}, u32[]{:S(2)}) collective-permute-start(bf16[256,1536]{1,0:T(8,128)(2,1)} %pad_maximum_fusion), channel_id=1, source_target_pairs={{0,12},{4,8},{8,4},{12,0},{1,13},{5,9},{9,5},{13,1},{2,14},{6,10},... | collective-permute-start | bytes 2359304 | tf_op jit(solution)/shard_map/ppermute | solution.py:21
  31.0 103.8 %collective-permute-start.22 = (bf16[256,1536]{1,0:T(8,128)(2,1)}, bf16[256,1536]{1,0:T(8,128)(2,1)S(1)}, u32[]{:S(2)}, u32[]{:S(2)}) collective-permute-start(bf16[256,1536]{1,0:T(8,128)(2,1)} %pad_maximum_fusion.1), channel_id=1, source_target_pairs={{0,8},{4,12},{8,0},{12,4},{1,9},{5,13},{9,1},{13,5},{2,10},{6,14},... | collective-permute-start | bytes 2359304 | tf_op jit(solution)/shard_map/ppermute | solution.py:21
  32.6 47.0 %collective-permute-start.28 = (bf16[384,512]{1,0:T(8,128)(2,1)}, bf16[384,512]{1,0:T(8,128)(2,1)S(1)}, u32[]{:S(2)}, u32[]{:S(2)}) collective-permute-start(bf16[384,512]{1,0:T(8,128)(2,1)} %get-tuple-element.32), channel_id=1, source_target_pairs={{0,4},{4,0},{8,12},{12,8},{1,5},{5,1},{9,13},{13,9},{2,6},{6,2},{1... | collective-permute-start | bytes 1179656 | tf_op jit(solution)/shard_map/ppermute | solution.py:21
  33.6 81.2 %collective-permute-start.30 = (bf16[384,512]{1,0:T(8,128)(2,1)}, bf16[384,512]{1,0:T(8,128)(2,1)S(1)}, u32[]{:S(2)}, u32[]{:S(2)}) collective-permute-start(bf16[384,512]{1,0:T(8,128)(2,1)} %get-tuple-element.31), channel_id=1, source_target_pairs={{0,8},{4,12},{8,0},{12,4},{1,9},{5,13},{9,1},{13,5},{2,10},{6,14},... | collective-permute-start | bytes 1179656 | tf_op jit(solution)/shard_map/ppermute | solution.py:21
  79.6 48.3 %collective-permute-start.26 = (bf16[384,512]{1,0:T(8,128)(2,1)}, bf16[384,512]{1,0:T(8,128)(2,1)S(1)}, u32[]{:S(2)}, u32[]{:S(2)}) collective-permute-start(bf16[384,512]{1,0:T(8,128)(2,1)} %get-tuple-element.32), channel_id=1, source_target_pairs={{0,12},{4,8},{8,4},{12,0},{1,13},{5,9},{9,5},{13,1},{2,14},{6,10},... | collective-permute-start | bytes 1179656 | tf_op jit(solution)/shard_map/ppermute | solution.py:21
  115.5 10.9 %collective-permute-start.16 = (bf16[16,512]{1,0:T(8,128)(2,1)S(1)}, bf16[16,512]{1,0:T(8,128)(2,1)S(1)}, u32[]{:S(2)}, u32[]{:S(2)}) collective-permute-start(bf16[16,512]{1,0:T(8,128)(2,1)S(1)} %slice_select_fusion), channel_id=1, source_target_pairs={{4,12},{8,0},{5,13},{9,1},{6,14},{10,2},{7,15},{11,3},{20,28},{24,... | collective-permute-start | bytes 49160 | tf_op jit(solution)/shard_map/ppermute | solution.py:21
  126.4 10.9 %collective-permute-start.11 = (bf16[512,512]{1,0:T(8,128)(2,1)S(1)}, bf16[512,512]{1,0:T(8,128)(2,1)S(1)}, u32[]{:S(2)}, u32[]{:S(2)}) collective-permute-start(bf16[512,512]{1,0:T(8,128)(2,1)S(1)} %multiply_convert_fusion.x0), channel_id=1, source_target_pairs={{0,4},{4,0},{8,12},{12,8},{1,5},{5,1},{9,13},{13,9},{2,6},{6,2},{1... | collective-permute-start | bytes 1572872 | tf_op jit(solution)/shard_map/ppermute | solution.py:21
  126.4 23.2 %collective-permute-start.21 = (bf16[256,1536]{1,0:T(8,128)(2,1)}, bf16[256,1536]{1,0:T(8,128)(2,1)S(1)}, u32[]{:S(2)}, u32[]{:S(2)}) collective-permute-start(bf16[256,1536]{1,0:T(8,128)(2,1)} %collective-permute-done.20.z1), channel_id=1, source_target_pairs={{0,16},{16,0},{1,17},{17,1},{2,18},{18,2},{3,19},{19,3},{4,20},{20... | collective-permute-start | bytes 2359304 | tf_op jit(solution)/shard_map/ppermute | solution.py:21
  134.2 14.8 %collective-permute-start.9 = (bf16[512,512]{1,0:T(8,128)(2,1)S(1)}, bf16[512,512]{1,0:T(8,128)(2,1)S(1)}, u32[]{:S(2)}, u32[]{:S(2)}) collective-permute-start(bf16[512,512]{1,0:T(8,128)(2,1)S(1)} %multiply_convert_fusion.x0), channel_id=1, source_target_pairs={{0,2},{1,3},{2,0},{3,1},{4,6},{5,7},{6,4},{7,5},{8,10},{9,11},{10,... | collective-permute-start | bytes 1572872 | tf_op jit(solution)/shard_map/ppermute | solution.py:21
  134.8 14.3 %collective-permute-start.8 = (bf16[512,512]{1,0:T(8,128)(2,1)S(1)}, bf16[512,512]{1,0:T(8,128)(2,1)S(1)}, u32[]{:S(2)}, u32[]{:S(2)}) collective-permute-start(bf16[512,512]{1,0:T(8,128)(2,1)S(1)} %multiply_convert_fusion.x0), channel_id=1, source_target_pairs={{0,1},{1,0},{2,3},{3,2},{4,5},{5,4},{6,7},{7,6},{8,9},{9,8},{10,11... | collective-permute-start | bytes 1572872 | tf_op jit(solution)/shard_map/ppermute | solution.py:21
  134.8 29.1 %collective-permute-start.23 = (bf16[256,1536]{1,0:T(8,128)(2,1)S(1)}, bf16[256,1536]{1,0:T(8,128)(2,1)S(1)}, u32[]{:S(2)}, u32[]{:S(2)}) collective-permute-start(bf16[256,1536]{1,0:T(8,128)(2,1)S(1)} %collective-permute-done.22.z2), channel_id=1, source_target_pairs={{0,16},{16,0},{1,17},{17,1},{2,18},{18,2},{3,19},{19,3},{4,20},{20... | collective-permute-start | bytes 2359304 | tf_op jit(solution)/shard_map/ppermute | solution.py:21
  137.3 22.2 %collective-permute-start.13 = (bf16[512,512]{1,0:T(8,128)(2,1)S(1)}, bf16[512,512]{1,0:T(8,128)(2,1)S(1)}, u32[]{:S(2)}, u32[]{:S(2)}) collective-permute-start(bf16[512,512]{1,0:T(8,128)(2,1)S(1)} %collective-permute-done.11.o0), channel_id=1, source_target_pairs={{0,2},{1,3},{2,0},{3,1},{4,6},{5,7},{6,4},{7,5},{8,10},{9,11},{10,... | collective-permute-start | bytes 1572872 | tf_op jit(solution)/shard_map/ppermute | solution.py:21
  149.0 16.3 %collective-permute-start.10 = (bf16[512,512]{1,0:T(8,128)(2,1)S(1)}, bf16[512,512]{1,0:T(8,128)(2,1)S(1)}, u32[]{:S(2)}, u32[]{:S(2)}) collective-permute-start(bf16[512,512]{1,0:T(8,128)(2,1)S(1)} %collective-permute-done.9.x2), channel_id=1, source_target_pairs={{0,1},{1,0},{2,3},{3,2},{4,5},{5,4},{6,7},{7,6},{8,9},{9,8},{10,11... | collective-permute-start | bytes 1572872 | tf_op jit(solution)/shard_map/ppermute | solution.py:21
  149.1 16.8 %collective-permute-start.12 = (bf16[512,512]{1,0:T(8,128)(2,1)S(1)}, bf16[512,512]{1,0:T(8,128)(2,1)S(1)}, u32[]{:S(2)}, u32[]{:S(2)}) collective-permute-start(bf16[512,512]{1,0:T(8,128)(2,1)S(1)} %collective-permute-done.11.o0), channel_id=1, source_target_pairs={{0,1},{1,0},{2,3},{3,2},{4,5},{5,4},{6,7},{7,6},{8,9},{9,8},{10,11... | collective-permute-start | bytes 1572872 | tf_op jit(solution)/shard_map/ppermute | solution.py:21
  149.6 31.2 %collective-permute-start.25 = (bf16[256,1536]{1,0:T(8,128)(2,1)S(1)}, bf16[256,1536]{1,0:T(8,128)(2,1)S(1)}, u32[]{:S(2)}, u32[]{:S(2)}) collective-permute-start(bf16[256,1536]{1,0:T(8,128)(2,1)S(1)} %collective-permute-done.24.z3), channel_id=1, source_target_pairs={{0,16},{16,0},{1,17},{17,1},{2,18},{18,2},{3,19},{19,3},{4,20},{20... | collective-permute-start | bytes 2359304 | tf_op jit(solution)/shard_map/ppermute | solution.py:21
  163.9 25.3 %collective-permute-start.29 = (bf16[384,512]{1,0:T(8,128)(2,1)S(1)}, bf16[384,512]{1,0:T(8,128)(2,1)S(1)}, u32[]{:S(2)}, u32[]{:S(2)}) collective-permute-start(bf16[384,512]{1,0:T(8,128)(2,1)S(1)} %collective-permute-done.28.z1), channel_id=1, source_target_pairs={{0,16},{16,0},{1,17},{17,1},{2,18},{18,2},{3,19},{19,3},{4,20},{20... | collective-permute-start | bytes 1179656 | tf_op jit(solution)/shard_map/ppermute | solution.py:21
  165.4 32.2 %collective-permute-start.31 = (bf16[384,512]{1,0:T(8,128)(2,1)S(1)}, bf16[384,512]{1,0:T(8,128)(2,1)S(1)}, u32[]{:S(2)}, u32[]{:S(2)}) collective-permute-start(bf16[384,512]{1,0:T(8,128)(2,1)S(1)} %collective-permute-done.30.z2), channel_id=1, source_target_pairs={{0,16},{16,0},{1,17},{17,1},{2,18},{18,2},{3,19},{19,3},{4,20},{20... | collective-permute-start | bytes 1179656 | tf_op jit(solution)/shard_map/ppermute | solution.py:21
  165.9 36.0 %collective-permute-start.27 = (bf16[384,512]{1,0:T(8,128)(2,1)S(1)}, bf16[384,512]{1,0:T(8,128)(2,1)S(1)}, u32[]{:S(2)}, u32[]{:S(2)}) collective-permute-start(bf16[384,512]{1,0:T(8,128)(2,1)S(1)} %collective-permute-done.26.z3), channel_id=1, source_target_pairs={{0,16},{16,0},{1,17},{17,1},{2,18},{18,2},{3,19},{19,3},{4,20},{20... | collective-permute-start | bytes 1179656 | tf_op jit(solution)/shard_map/ppermute | solution.py:21
  207.8 9.2 %collective-permute-start.35 = (bf16[256,512]{1,0:T(8,128)(2,1)S(1)}, bf16[256,512]{1,0:T(8,128)(2,1)S(1)}, u32[]{:S(2)}, u32[]{:S(2)}) collective-permute-start(bf16[256,512]{1,0:T(8,128)(2,1)S(1)} %get-tuple-element.30), channel_id=1, source_target_pairs={{0,2},{1,3},{2,0},{3,1},{4,6},{5,7},{6,4},{7,5},{8,10},{9,11},{10,... | collective-permute-start | bytes 786440 | tf_op jit(solution)/shard_map/ppermute | solution.py:21
  208.6 14.9 %collective-permute-start.37 = (bf16[2,256,512]{2,1,0:T(8,128)(2,1)S(1)}, bf16[2,256,512]{2,1,0:T(8,128)(2,1)S(1)}, u32[]{:S(2)}, u32[]{:S(2)}) collective-permute-start(bf16[2,256,512]{2,1,0:T(8,128)(2,1)S(1)} %pad_maximum_fusion.2), channel_id=1, source_target_pairs={{0,4},{4,0},{8,12},{12,8},{1,5},{5,1},{9,13},{13,9},{2,6},{6,2},{1... | collective-permute-start | bytes 1572872 | tf_op jit(solution)/shard_map/ppermute | solution.py:21
  210.4 13.2 %collective-permute-start.33 = (bf16[256,512]{1,0:T(8,128)(2,1)S(1)}, bf16[256,512]{1,0:T(8,128)(2,1)S(1)}, u32[]{:S(2)}, u32[]{:S(2)}) collective-permute-start(bf16[256,512]{1,0:T(8,128)(2,1)S(1)} %get-tuple-element.29), channel_id=1, source_target_pairs={{0,2},{1,3},{2,0},{3,1},{4,6},{5,7},{6,4},{7,5},{8,10},{9,11},{10,... | collective-permute-start | bytes 786440 | tf_op jit(solution)/shard_map/ppermute | solution.py:21
  217.1 10.8 %collective-permute-start.36 = (bf16[256,512]{1,0:T(8,128)(2,1)S(1)}, bf16[256,512]{1,0:T(8,128)(2,1)S(1)}, u32[]{:S(2)}, u32[]{:S(2)}) collective-permute-start(bf16[256,512]{1,0:T(8,128)(2,1)S(1)} %fusion.15), channel_id=1, source_target_pairs={{0,4},{4,0},{8,12},{12,8},{1,5},{5,1},{9,13},{13,9},{2,6},{6,2},{1... | collective-permute-start | bytes 786440 | tf_op jit(solution)/shard_map/ppermute | solution.py:21
  (24 other events, 526.3 us)

commit v4 on v3

--- a/solution.py
+++ b/solution.py
@@ -12,6 +12,7 @@
 WINDOW = 128
 CONV = 3
 HALO = 16
+MIDDLE = 9
 
 
 SWAP = [(0, 1), (1, 0)]
@@ -37,8 +38,14 @@
     both = jnp.stack([own_keys, own_values])
     up = [(i, i + 1) for i in range(levels - 1)]
     down = [(i + 1, i) for i in range(levels - 1)]
-    before = send(both[:, tokens - WINDOW :], "sp", up)
-    after = send(both[:, :WINDOW], "sp", down)
+
+    def rows_of(start):
+        return jnp.stack(
+            [lax.dynamic_slice(cells, (start, kv_head * HD), (WINDOW, HD)) for cells in (keys, values)]
+        )
+
+    before = send(rows_of(tokens - WINDOW), "sp", up)
+    after = send(rows_of(0), "sp", down)
     extended = jnp.concatenate([before, both, after], axis=1)
     span = tokens + 2 * WINDOW
     q_heads = queries.reshape(tokens, heads_here, HD)
@@ -541,7 +548,7 @@
     away_other, away_own, here = down(act, w_down, dn)
     came = [send(away_other, "tp", xor_pairs(4, 1)), send(away_own, "tp", xor_pairs(4, 1))]
 
-    middle = tokens // 2
+    middle = tokens // 16 * MIDDLE
 
     def partial(which, slot, rows):
         return here[which, slot, rows].astype(jnp.float32) + came[which][slot, rows].astype(jnp.float32)
@@ -552,7 +559,7 @@
     top, low = slice(0, middle), slice(middle, tokens)
     x_other = cross(partial(0, 1, top), "tp", 2)
     z_low = cross(jnp.stack([partial(0, 0, low), partial(0, 1, low)]), "sp", 1)
-    x_top = cross(partial(1, 1, top), "tp", 2)
+    x_top = cross(partial(1, 1, slice(0, middle + HALO)), "tp", 2)[:middle]
     back = cross(partial(0, 0, top) + x_other, "sp", 1)
     low_sum = (partial(1, 1, low) + z_low[1]).astype(jnp.bfloat16)
     x_low = cross(low_sum, "tp", 2)

time: 237 us -> 228 us (0.962)
  waiting for transfers between devices: 160 us -> 152 us
    ppermute x39, waiting for transfers between devices: 160 us -> 152 us  [send(): return lax.ppermute(cells, axis, pairs)]
  transfers between devices with their start and end apart: 39 -> 39, of which waited for: 22 -> 22; matrix products, arithmetic and copies ran while one was open for 5% -> 5% of each run, Pallas kernels for 7% -> 8%
where the time goes in v4:
time: 228 us
  waiting for transfers between devices  152 us (67%)
  starting transfers between devices  39 us (17%)
  Pallas kernels  18.9 us (8%)
  other arithmetic  6.99 us (3%)
  local copies, waits for them, and re-layouts  5.97 us (3%)
  matrix products  4.83 us (2%)
    ppermute x39, waiting for transfers between devices, send(): return lax.ppermute(cells, axis, pairs)  152 us
    ppermute x39, starting transfers between devices, send(): return lax.ppermute(cells, axis, pairs)  39 us
    pallas_call x1, Pallas kernels, gate_up(): pl.pallas_call(gate_up_kernel, out_shape=(jax.ShapeDtypeStruct((2 * token...  8.18 us
    pallas_call x1, Pallas kernels, activate_last(): pl.pallas_call(activate_kernel, out_shape=jax.ShapeDtypeStruct((acc.shape...  4.98 us
  transfers between devices with their start and end apart: 39, of which 22 were waited for; matrix products, arithmetic and copies ran while one was open for 5% of the time, Pallas kernels for 8%

profile of v4, /device:TPU:0, one launch (start us, length us, event | category | flops | bytes accessed | tf_op | source)
XLA Modules:
  0.0 228.1 jit_solution(9768513565378511265)
XLA Ops:
  1.0 5.0 %collective-permute-start = (bf16[2,128,128]{2,1,0:T(8,128)(2,1)S(1)}, bf16[2,128,128]{2,1,0:T(8,128)(2,1)S(1)}, u32[]{:S(2)}, u32[]{:S(2)}) collective-permute-start(bf16[2,128,128]{2,1,0:T(8,128)(2,1)S(1)} %pad_maximum_fusion.4), channel_id=1, source_target_pairs={{0,4},{4,8},{8,12},{1,5},{5,9},{9,13},{2,6},{6,10},{10,14},{3,7},{... | collective-permute-start | bytes 196616 | tf_op jit(solution)/shard_map/ppermute | solution.py:22
  9.7 2.4 %collective-permute-done.1 = bf16[2,128,128]{2,1,0:T(8,128)(2,1)S(1)} collective-permute-done((bf16[2,128,128]{2,1,0:T(8,128)(2,1)S(1)}, bf16[2,128,128]{2,1,0:T(8,128)(2,1)S(1)}, u32[]{:S(2)}, u32[]{:S(2)}) %collective-permute-start.1) | collective-permute-done | bytes 65568 | tf_op jit(solution)/shard_map/ppermute | solution.py:22
  19.1 2.5 %collective-permute-start.24 = (bf16[256,1536]{1,0:T(8,128)(2,1)}, bf16[256,1536]{1,0:T(8,128)(2,1)S(1)}, u32[]{:S(2)}, u32[]{:S(2)}) collective-permute-start(bf16[256,1536]{1,0:T(8,128)(2,1)} %pad_maximum_fusion), channel_id=1, source_target_pairs={{0,12},{4,8},{8,4},{12,0},{1,13},{5,9},{9,5},{13,1},{2,14},{6,10},... | collective-permute-start | bytes 2359304 | tf_op jit(solution)/shard_map/ppermute | solution.py:22
  24.2 2.9 %fusion.26 = (f32[512]{0:T(512)S(1)}, f32[512]{0:T(512)S(1)}, f32[512,512]{1,0:T(8,128)}) fusion(bf16[512,1024]{0,1:T(8,128)(2,1)S(1)} %constant_dynamic-update-slice_fusion.2, bf16[1024,512]{1,0:T(8,128)(2,1)S(1)} %copy-done, bf16[512,2048]{1,0:T(8,128)(2,1)} %param.16, s32[]{:T(128)S(6)} %select_n.68), kind=kOutput, calls=%fused_computation.83 | convolution fusion | flops 538180608 | bytes 3674116 | tf_op jit(solution)/shard_map/dot_general | solution.py:97
  35.9 43.6 %collective-permute-done.28.z1 = bf16[384,512]{1,0:T(8,128)(2,1)S(1)} collective-permute-done((bf16[384,512]{1,0:T(8,128)(2,1)}, bf16[384,512]{1,0:T(8,128)(2,1)S(1)}, u32[]{:S(2)}, u32[]{:S(2)}) %collective-permute-start.28) | collective-permute-done | bytes 393248 | tf_op jit(solution)/shard_map/ppermute | solution.py:22
  79.5 2.5 %collective-permute-start.26 = (bf16[384,512]{1,0:T(8,128)(2,1)}, bf16[384,512]{1,0:T(8,128)(2,1)S(1)}, u32[]{:S(2)}, u32[]{:S(2)}) collective-permute-start(bf16[384,512]{1,0:T(8,128)(2,1)} %get-tuple-element.28), channel_id=1, source_target_pairs={{0,12},{4,8},{8,4},{12,0},{1,13},{5,9},{9,5},{13,1},{2,14},{6,10},... | collective-permute-start | bytes 1179656 | tf_op jit(solution)/shard_map/ppermute | solution.py:22
  82.0 33.0 %collective-permute-done.30.z2 = bf16[384,512]{1,0:T(8,128)(2,1)S(1)} collective-permute-done((bf16[384,512]{1,0:T(8,128)(2,1)}, bf16[384,512]{1,0:T(8,128)(2,1)S(1)}, u32[]{:S(2)}, u32[]{:S(2)}) %collective-permute-start.30) | collective-permute-done | bytes 393248 | tf_op jit(solution)/shard_map/ppermute | solution.py:22
  117.1 9.3 %collective-permute-done.16 = bf16[16,512]{1,0:T(8,128)(2,1)S(1)} collective-permute-done((bf16[16,512]{1,0:T(8,128)(2,1)S(1)}, bf16[16,512]{1,0:T(8,128)(2,1)S(1)}, u32[]{:S(2)}, u32[]{:S(2)}) %collective-permute-start.16) | collective-permute-done | bytes 16416 | tf_op jit(solution)/shard_map/ppermute | solution.py:22
  128.5 3.4 %collective-permute-done.18.e2 = bf16[32,512]{1,0:T(8,128)(2,1)S(1)} collective-permute-done((bf16[32,512]{1,0:T(8,128)(2,1)S(1)}, bf16[32,512]{1,0:T(8,128)(2,1)S(1)}, u32[]{:S(2)}, u32[]{:S(2)}) %collective-permute-start.18) | collective-permute-done | bytes 32800 | tf_op jit(solution)/shard_map/ppermute | solution.py:22
  135.4 1.9 collective-permute-done.11.o0
  137.8 11.2 %collective-permute-done.9.x2 = bf16[512,512]{1,0:T(8,128)(2,1)S(1)} collective-permute-done((bf16[512,512]{1,0:T(8,128)(2,1)S(1)}, bf16[512,512]{1,0:T(8,128)(2,1)S(1)}, u32[]{:S(2)}, u32[]{:S(2)}) %collective-permute-start.9) | collective-permute-done | bytes 524320 | tf_op jit(solution)/shard_map/ppermute | solution.py:22
  150.1 9.4 %collective-permute-done.13.o2 = bf16[512,512]{1,0:T(8,128)(2,1)S(1)} collective-permute-done((bf16[512,512]{1,0:T(8,128)(2,1)S(1)}, bf16[512,512]{1,0:T(8,128)(2,1)S(1)}, u32[]{:S(2)}, u32[]{:S(2)}) %collective-permute-start.13) | collective-permute-done | bytes 524320 | tf_op jit(solution)/shard_map/ppermute | solution.py:22
  159.5 4.4 %collective-permute-done.23.y2 = bf16[256,1536]{1,0:T(8,128)(2,1)S(1)} collective-permute-done((bf16[256,1536]{1,0:T(8,128)(2,1)S(1)}, bf16[256,1536]{1,0:T(8,128)(2,1)S(1)}, u32[]{:S(2)}, u32[]{:S(2)}) %collective-permute-start.23) | collective-permute-done | bytes 786464 | tf_op jit(solution)/shard_map/ppermute | solution.py:22
  169.0 8.2 %gate_up.1 = (f32[1024,1536]{1,0:T(8,128)S(1)}, f32[32,768]{1,0:T(8,128)S(1)}, bf16[1056,512]{1,0:T(8,128)(2,1)S(1)}) custom-call(bf16[512,512]{1,0:T(8,128)(2,1)S(1)} %multiply_convert_fusion.x0, bf16[512,512]{1,0:T(8,128)(2,1)S(1)} %collective-permute-done.8.x1, bf16[512,512]{1,0:T(8,128)(2,1)S(1)} %collective-permute-done.9.x2, ...), custom_call_target="tpu_custom_call" | custom-call | tf_op jit(solution)/shard_map/gate_up/pallas_call | solution.py:292
  177.1 3.6 %collective-permute-done.25.y3 = bf16[256,1536]{1,0:T(8,128)(2,1)S(1)} collective-permute-done((bf16[256,1536]{1,0:T(8,128)(2,1)S(1)}, bf16[256,1536]{1,0:T(8,128)(2,1)S(1)}, u32[]{:S(2)}, u32[]{:S(2)}) %collective-permute-start.25) | collective-permute-done | bytes 786464 | tf_op jit(solution)/shard_map/ppermute | solution.py:22
  180.7 5.0 %activate.1.act = bf16[1024,768]{1,0:T(8,128)(2,1)S(1)} custom-call(f32[1024,1536]{1,0:T(8,128)S(1)} %get-tuple-element.14.acc, f32[32,768]{1,0:T(8,128)S(1)} %get-tuple-element.15.around, bf16[1056,512]{1,0:T(8,128)(2,1)S(1)} %get-tuple-element.16.last, bf16[256,1536]{1,0:T(8,128)(2,1)S(1)} %collective-permute-done.24.z3, ...), custom_call_target="tpu_custom_call" | custom-call | tf_op jit(solution)/shard_map/activate/pallas_call | solution.py:364
  185.7 3.4 %collective-permute-done.29.y1 = bf16[384,512]{1,0:T(8,128)(2,1)S(1)} collective-permute-done((bf16[384,512]{1,0:T(8,128)(2,1)S(1)}, bf16[384,512]{1,0:T(8,128)(2,1)S(1)}, u32[]{:S(2)}, u32[]{:S(2)}) %collective-permute-start.29) | collective-permute-done | bytes 393248 | tf_op jit(solution)/shard_map/ppermute | solution.py:22
  189.1 8.4 %collective-permute-done.31.y2 = bf16[384,512]{1,0:T(8,128)(2,1)S(1)} collective-permute-done((bf16[384,512]{1,0:T(8,128)(2,1)S(1)}, bf16[384,512]{1,0:T(8,128)(2,1)S(1)}, u32[]{:S(2)}, u32[]{:S(2)}) %collective-permute-start.31) | collective-permute-done | bytes 393248 | tf_op jit(solution)/shard_map/ppermute | solution.py:22
  197.6 4.3 %down.1 = (bf16[2,512,512]{2,1,0:T(8,128)(2,1)S(1)}, bf16[2,512,512]{2,1,0:T(8,128)(2,1)S(1)}, bf16[2,2,512,512]{3,2,1,0:T(8,128)(2,1)S(1)}) custom-call(bf16[1024,768]{1,0:T(8,128)(2,1)S(1)} %activate.1.act, bf16[1536,512]{1,0:T(8,128)(2,1)S(1)} %copy-done.1, bf16[384,512]{1,0:T(8,128)(2,1)S(1)} %collective-permute-done.28.z1, ...), custom_call_target="tpu_custom_call" | custom-call | tf_op jit(solution)/shard_map/down/pallas_call | solution.py:473
  204.0 2.1 collective-permute-done.34
  210.5 5.6 %collective-permute-done.35 = bf16[288,512]{1,0:T(8,128)(2,1)S(1)} collective-permute-done((bf16[288,512]{1,0:T(8,128)(2,1)S(1)}, bf16[288,512]{1,0:T(8,128)(2,1)S(1)}, u32[]{:S(2)}, u32[]{:S(2)}) %collective-permute-start.35) | collective-permute-done | bytes 294944 | tf_op jit(solution)/shard_map/ppermute | solution.py:22
  216.3 1.9 collective-permute-start.36
  218.2 2.3 collective-permute-done.37
  222.8 2.9 %collective-permute-done.36 = bf16[288,512]{1,0:T(8,128)(2,1)S(1)} collective-permute-done((bf16[288,512]{1,0:T(8,128)(2,1)S(1)}, bf16[288,512]{1,0:T(8,128)(2,1)S(1)}, u32[]{:S(2)}, u32[]{:S(2)}) %collective-permute-start.36) | collective-permute-done | bytes 294944 | tf_op jit(solution)/shard_map/ppermute | solution.py:22
  (126 shorter events, 48.5 us)
Async XLA Ops:
  1.0 8.7 %collective-permute-start = (bf16[2,128,128]{2,1,0:T(8,128)(2,1)S(1)}, bf16[2,128,128]{2,1,0:T(8,128)(2,1)S(1)}, u32[]{:S(2)}, u32[]{:S(2)}) collective-permute-start(bf16[2,128,128]{2,1,0:T(8,128)(2,1)S(1)} %pad_maximum_fusion.4), channel_id=1, source_target_pairs={{0,4},{4,8},{8,12},{1,5},{5,9},{9,13},{2,6},{6,10},{10,14},{3,7},{... | collective-permute-start | bytes 196616 | tf_op jit(solution)/shard_map/ppermute | solution.py:22
  17.5 108.9 %collective-permute-start.20 = (bf16[256,1536]{1,0:T(8,128)(2,1)}, bf16[256,1536]{1,0:T(8,128)(2,1)}, u32[]{:S(2)}, u32[]{:S(2)}) collective-permute-start(bf16[256,1536]{1,0:T(8,128)(2,1)} %pad_maximum_fusion), channel_id=1, source_target_pairs={{0,4},{4,0},{8,12},{12,8},{1,5},{5,1},{9,13},{13,9},{2,6},{6,2},{1... | collective-permute-start | bytes 2359304 | tf_op jit(solution)/shard_map/ppermute | solution.py:22
  19.1 115.7 %collective-permute-start.24 = (bf16[256,1536]{1,0:T(8,128)(2,1)}, bf16[256,1536]{1,0:T(8,128)(2,1)S(1)}, u32[]{:S(2)}, u32[]{:S(2)}) collective-permute-start(bf16[256,1536]{1,0:T(8,128)(2,1)} %pad_maximum_fusion), channel_id=1, source_target_pairs={{0,12},{4,8},{8,4},{12,0},{1,13},{5,9},{9,5},{13,1},{2,14},{6,10},... | collective-permute-start | bytes 2359304 | tf_op jit(solution)/shard_map/ppermute | solution.py:22
  30.9 103.9 %collective-permute-start.22 = (bf16[256,1536]{1,0:T(8,128)(2,1)}, bf16[256,1536]{1,0:T(8,128)(2,1)S(1)}, u32[]{:S(2)}, u32[]{:S(2)}) collective-permute-start(bf16[256,1536]{1,0:T(8,128)(2,1)} %pad_maximum_fusion.1), channel_id=1, source_target_pairs={{0,8},{4,12},{8,0},{12,4},{1,9},{5,13},{9,1},{13,5},{2,10},{6,14},... | collective-permute-start | bytes 2359304 | tf_op jit(solution)/shard_map/ppermute | solution.py:22
  32.5 47.0 %collective-permute-start.28 = (bf16[384,512]{1,0:T(8,128)(2,1)}, bf16[384,512]{1,0:T(8,128)(2,1)S(1)}, u32[]{:S(2)}, u32[]{:S(2)}) collective-permute-start(bf16[384,512]{1,0:T(8,128)(2,1)} %get-tuple-element.28), channel_id=1, source_target_pairs={{0,4},{4,0},{8,12},{12,8},{1,5},{5,1},{9,13},{13,9},{2,6},{6,2},{1... | collective-permute-start | bytes 1179656 | tf_op jit(solution)/shard_map/ppermute | solution.py:22
  33.6 81.3 %collective-permute-start.30 = (bf16[384,512]{1,0:T(8,128)(2,1)}, bf16[384,512]{1,0:T(8,128)(2,1)S(1)}, u32[]{:S(2)}, u32[]{:S(2)}) collective-permute-start(bf16[384,512]{1,0:T(8,128)(2,1)} %get-tuple-element.27), channel_id=1, source_target_pairs={{0,8},{4,12},{8,0},{12,4},{1,9},{5,13},{9,1},{13,5},{2,10},{6,14},... | collective-permute-start | bytes 1179656 | tf_op jit(solution)/shard_map/ppermute | solution.py:22
  79.5 48.4 %collective-permute-start.26 = (bf16[384,512]{1,0:T(8,128)(2,1)}, bf16[384,512]{1,0:T(8,128)(2,1)S(1)}, u32[]{:S(2)}, u32[]{:S(2)}) collective-permute-start(bf16[384,512]{1,0:T(8,128)(2,1)} %get-tuple-element.28), channel_id=1, source_target_pairs={{0,12},{4,8},{8,4},{12,0},{1,13},{5,9},{9,5},{13,1},{2,14},{6,10},... | collective-permute-start | bytes 1179656 | tf_op jit(solution)/shard_map/ppermute | solution.py:22
  115.6 10.8 %collective-permute-start.16 = (bf16[16,512]{1,0:T(8,128)(2,1)S(1)}, bf16[16,512]{1,0:T(8,128)(2,1)S(1)}, u32[]{:S(2)}, u32[]{:S(2)}) collective-permute-start(bf16[16,512]{1,0:T(8,128)(2,1)S(1)} %slice_select_fusion), channel_id=1, source_target_pairs={{4,12},{8,0},{5,13},{9,1},{6,14},{10,2},{7,15},{11,3},{20,28},{24,... | collective-permute-start | bytes 49160 | tf_op jit(solution)/shard_map/ppermute | solution.py:22
  126.4 10.9 %collective-permute-start.11 = (bf16[512,512]{1,0:T(8,128)(2,1)S(1)}, bf16[512,512]{1,0:T(8,128)(2,1)S(1)}, u32[]{:S(2)}, u32[]{:S(2)}) collective-permute-start(bf16[512,512]{1,0:T(8,128)(2,1)S(1)} %multiply_convert_fusion.x0), channel_id=1, source_target_pairs={{0,4},{4,0},{8,12},{12,8},{1,5},{5,1},{9,13},{13,9},{2,6},{6,2},{1... | collective-permute-start | bytes 1572872 | tf_op jit(solution)/shard_map/ppermute | solution.py:22
  126.4 23.2 %collective-permute-start.21 = (bf16[256,1536]{1,0:T(8,128)(2,1)}, bf16[256,1536]{1,0:T(8,128)(2,1)S(1)}, u32[]{:S(2)}, u32[]{:S(2)}) collective-permute-start(bf16[256,1536]{1,0:T(8,128)(2,1)} %collective-permute-done.20.z1), channel_id=1, source_target_pairs={{0,16},{16,0},{1,17},{17,1},{2,18},{18,2},{3,19},{19,3},{4,20},{20... | collective-permute-start | bytes 2359304 | tf_op jit(solution)/shard_map/ppermute | solution.py:22
  134.3 14.8 %collective-permute-start.9 = (bf16[512,512]{1,0:T(8,128)(2,1)S(1)}, bf16[512,512]{1,0:T(8,128)(2,1)S(1)}, u32[]{:S(2)}, u32[]{:S(2)}) collective-permute-start(bf16[512,512]{1,0:T(8,128)(2,1)S(1)} %multiply_convert_fusion.x0), channel_id=1, source_target_pairs={{0,2},{1,3},{2,0},{3,1},{4,6},{5,7},{6,4},{7,5},{8,10},{9,11},{10,... | collective-permute-start | bytes 1572872 | tf_op jit(solution)/shard_map/ppermute | solution.py:22
  134.8 14.3 %collective-permute-start.8 = (bf16[512,512]{1,0:T(8,128)(2,1)S(1)}, bf16[512,512]{1,0:T(8,128)(2,1)S(1)}, u32[]{:S(2)}, u32[]{:S(2)}) collective-permute-start(bf16[512,512]{1,0:T(8,128)(2,1)S(1)} %multiply_convert_fusion.x0), channel_id=1, source_target_pairs={{0,1},{1,0},{2,3},{3,2},{4,5},{5,4},{6,7},{7,6},{8,9},{9,8},{10,11... | collective-permute-start | bytes 1572872 | tf_op jit(solution)/shard_map/ppermute | solution.py:22
  134.8 29.1 %collective-permute-start.23 = (bf16[256,1536]{1,0:T(8,128)(2,1)S(1)}, bf16[256,1536]{1,0:T(8,128)(2,1)S(1)}, u32[]{:S(2)}, u32[]{:S(2)}) collective-permute-start(bf16[256,1536]{1,0:T(8,128)(2,1)S(1)} %collective-permute-done.22.z2), channel_id=1, source_target_pairs={{0,16},{16,0},{1,17},{17,1},{2,18},{18,2},{3,19},{19,3},{4,20},{20... | collective-permute-start | bytes 2359304 | tf_op jit(solution)/shard_map/ppermute | solution.py:22
  137.3 22.2 %collective-permute-start.13 = (bf16[512,512]{1,0:T(8,128)(2,1)S(1)}, bf16[512,512]{1,0:T(8,128)(2,1)S(1)}, u32[]{:S(2)}, u32[]{:S(2)}) collective-permute-start(bf16[512,512]{1,0:T(8,128)(2,1)S(1)} %collective-permute-done.11.o0), channel_id=1, source_target_pairs={{0,2},{1,3},{2,0},{3,1},{4,6},{5,7},{6,4},{7,5},{8,10},{9,11},{10,... | collective-permute-start | bytes 1572872 | tf_op jit(solution)/shard_map/ppermute | solution.py:22
  149.1 16.3 %collective-permute-start.10 = (bf16[512,512]{1,0:T(8,128)(2,1)S(1)}, bf16[512,512]{1,0:T(8,128)(2,1)S(1)}, u32[]{:S(2)}, u32[]{:S(2)}) collective-permute-start(bf16[512,512]{1,0:T(8,128)(2,1)S(1)} %collective-permute-done.9.x2), channel_id=1, source_target_pairs={{0,1},{1,0},{2,3},{3,2},{4,5},{5,4},{6,7},{7,6},{8,9},{9,8},{10,11... | collective-permute-start | bytes 1572872 | tf_op jit(solution)/shard_map/ppermute | solution.py:22
  149.1 16.8 %collective-permute-start.12 = (bf16[512,512]{1,0:T(8,128)(2,1)S(1)}, bf16[512,512]{1,0:T(8,128)(2,1)S(1)}, u32[]{:S(2)}, u32[]{:S(2)}) collective-permute-start(bf16[512,512]{1,0:T(8,128)(2,1)S(1)} %collective-permute-done.11.o0), channel_id=1, source_target_pairs={{0,1},{1,0},{2,3},{3,2},{4,5},{5,4},{6,7},{7,6},{8,9},{9,8},{10,11... | collective-permute-start | bytes 1572872 | tf_op jit(solution)/shard_map/ppermute | solution.py:22
  149.6 31.1 %collective-permute-start.25 = (bf16[256,1536]{1,0:T(8,128)(2,1)S(1)}, bf16[256,1536]{1,0:T(8,128)(2,1)S(1)}, u32[]{:S(2)}, u32[]{:S(2)}) collective-permute-start(bf16[256,1536]{1,0:T(8,128)(2,1)S(1)} %collective-permute-done.24.z3), channel_id=1, source_target_pairs={{0,16},{16,0},{1,17},{17,1},{2,18},{18,2},{3,19},{19,3},{4,20},{20... | collective-permute-start | bytes 2359304 | tf_op jit(solution)/shard_map/ppermute | solution.py:22
  163.9 25.3 %collective-permute-start.29 = (bf16[384,512]{1,0:T(8,128)(2,1)S(1)}, bf16[384,512]{1,0:T(8,128)(2,1)S(1)}, u32[]{:S(2)}, u32[]{:S(2)}) collective-permute-start(bf16[384,512]{1,0:T(8,128)(2,1)S(1)} %collective-permute-done.28.z1), channel_id=1, source_target_pairs={{0,16},{16,0},{1,17},{17,1},{2,18},{18,2},{3,19},{19,3},{4,20},{20... | collective-permute-start | bytes 1179656 | tf_op jit(solution)/shard_map/ppermute | solution.py:22
  165.4 32.2 %collective-permute-start.31 = (bf16[384,512]{1,0:T(8,128)(2,1)S(1)}, bf16[384,512]{1,0:T(8,128)(2,1)S(1)}, u32[]{:S(2)}, u32[]{:S(2)}) collective-permute-start(bf16[384,512]{1,0:T(8,128)(2,1)S(1)} %collective-permute-done.30.z2), channel_id=1, source_target_pairs={{0,16},{16,0},{1,17},{17,1},{2,18},{18,2},{3,19},{19,3},{4,20},{20... | collective-permute-start | bytes 1179656 | tf_op jit(solution)/shard_map/ppermute | solution.py:22
  165.9 36.0 %collective-permute-start.27 = (bf16[384,512]{1,0:T(8,128)(2,1)S(1)}, bf16[384,512]{1,0:T(8,128)(2,1)S(1)}, u32[]{:S(2)}, u32[]{:S(2)}) collective-permute-start(bf16[384,512]{1,0:T(8,128)(2,1)S(1)} %collective-permute-done.26.z3), channel_id=1, source_target_pairs={{0,16},{16,0},{1,17},{17,1},{2,18},{18,2},{3,19},{19,3},{4,20},{20... | collective-permute-start | bytes 1179656 | tf_op jit(solution)/shard_map/ppermute | solution.py:22
  206.2 9.9 %collective-permute-start.35 = (bf16[288,512]{1,0:T(8,128)(2,1)S(1)}, bf16[288,512]{1,0:T(8,128)(2,1)S(1)}, u32[]{:S(2)}, u32[]{:S(2)}) collective-permute-start(bf16[288,512]{1,0:T(8,128)(2,1)S(1)} %fusion.8), channel_id=1, source_target_pairs={{0,2},{1,3},{2,0},{3,1},{4,6},{5,7},{6,4},{7,5},{8,10},{9,11},{10,... | collective-permute-start | bytes 884744 | tf_op jit(solution)/shard_map/ppermute | solution.py:22
  207.0 13.5 %collective-permute-start.37 = (bf16[2,224,512]{2,1,0:T(8,128)(2,1)S(1)}, bf16[2,224,512]{2,1,0:T(8,128)(2,1)S(1)}, u32[]{:S(2)}, u32[]{:S(2)}) collective-permute-start(bf16[2,224,512]{2,1,0:T(8,128)(2,1)S(1)} %pad_maximum_fusion.2), channel_id=1, source_target_pairs={{0,4},{4,0},{8,12},{12,8},{1,5},{5,1},{9,13},{13,9},{2,6},{6,2},{1... | collective-permute-start | bytes 1376264 | tf_op jit(solution)/shard_map/ppermute | solution.py:22
  208.9 13.9 %collective-permute-start.33 = (bf16[304,512]{1,0:T(8,128)(2,1)S(1)}, bf16[304,512]{1,0:T(8,128)(2,1)S(1)}, u32[]{:S(2)}, u32[]{:S(2)}) collective-permute-start(bf16[304,512]{1,0:T(8,128)(2,1)S(1)} %fusion.7), channel_id=1, source_target_pairs={{0,2},{1,3},{2,0},{3,1},{4,6},{5,7},{6,4},{7,5},{8,10},{9,11},{10,... | collective-permute-start | bytes 933896 | tf_op jit(solution)/shard_map/ppermute | solution.py:22
  216.3 9.4 %collective-permute-start.36 = (bf16[288,512]{1,0:T(8,128)(2,1)S(1)}, bf16[288,512]{1,0:T(8,128)(2,1)S(1)}, u32[]{:S(2)}, u32[]{:S(2)}) collective-permute-start(bf16[288,512]{1,0:T(8,128)(2,1)S(1)} %fusion.10), channel_id=1, source_target_pairs={{0,4},{4,0},{8,12},{12,8},{1,5},{5,1},{9,13},{13,9},{2,6},{6,2},{1... | collective-permute-start | bytes 884744 | tf_op jit(solution)/shard_map/ppermute | solution.py:22
  (26 other events, 539.7 us)
